TPU v7x, 1024 devices: a whole 4x8x16 slice. The times are simulated.
1024 devices in a mesh: sp: 16 (over z), tp: 64 (over y, x, core).
Axes of the slice: x: 4, y: 8, z: 16, core: 2. Of those that a mesh axis runs over, the one named last changes fastest.
Arguments:
- latent: bfloat16 [4096, 4096], P(('sp', 'tp')), may hold values from -16 to 16
- context: bfloat16 [256, 4096], P('sp'), may hold values from -16 to 16
- cond: bfloat16 [4096], P('sp'), may hold values from -6 to 6
- cond_ctx: bfloat16 [4096], P('sp'), may hold values from -6 to 6
- mod_shift_w: bfloat16 [4096, 4096], P('sp', 'tp'), may hold values from -0.15625 to 0.15625
- mod_scale_w: bfloat16 [4096, 4096], P('sp', 'tp'), may hold values from -0.15625 to 0.15625
- mod_gate_w: bfloat16 [4096, 4096], P('sp', 'tp'), may hold values from -0.15625 to 0.15625
- norm_gain: bfloat16 [4096], replicated, may hold values from 0.099609375 to 1.8984375
- proj_z: bfloat16 [4096, 4096], P(None, 'tp'), may hold values from -0.09375 to 0.09375
- proj_x: bfloat16 [4096, 4096], P(None, 'tp'), may hold values from -0.09375 to 0.09375
- proj_b: bfloat16 [4096, 8192], P(None, 'tp'), may hold values from -0.09375 to 0.09375
- proj_c: bfloat16 [4096, 8192], P(None, 'tp'), may hold values from -0.09375 to 0.09375
- proj_dt: bfloat16 [4096, 128], replicated, may hold values from -0.09375 to 0.09375
- conv_x: bfloat16 [3, 4096], P(None, 'tp'), may hold values from -3.5 to 3.5
- conv_b: bfloat16 [3, 8192], P(None, 'tp'), may hold values from -3.5 to 3.5
- conv_c: bfloat16 [3, 8192], P(None, 'tp'), may hold values from -3.5 to 3.5
- dt_bias: float32 [128], P('tp'), may hold values from -1 to 1
- decay_log: float32 [128], P('tp'), may hold values from -11.6 to -2.9
- head_gain: bfloat16 [4096], P('tp'), may hold values from 0.099609375 to 1.8984375
- proj_out: bfloat16 [4096, 4096], P(None, 'tp'), may hold values from -0.09375 to 0.09375
Outputs:
- mixed: bfloat16 [4096, 4096], P(('sp', 'tp'))
All inputs are finite; a program needn't handle non-finite values.
Results may differ from a plain program's by a relative error of at most 0.0065.
Values may be sent and summed in bfloat16 or wider, within the bound.
A program may use at most 64 MiB of HBM per device.

v0:
```python
import jax
import jax.numpy as jnp
from jax import lax
from jax.sharding import Mesh
from jax.sharding import PartitionSpec as P

HEAD_DIM = 64
BLOCK = 128
TP = ("tp_0", "tp_1", "tp_2")
SP_TP = ("sp", "tp_0", "tp_1", "tp_2")


EPS = 1e-06


def copy_for_each(array, axis):
    copies = jnp.broadcast_to(array, (lax.axis_size(axis), *array.shape))
    return lax.all_to_all(copies, axis, split_axis=0, concat_axis=0, tiled=True)


def over_copies(array, axis):
    everything = copy_for_each(array, axis)
    return jnp.sum(everything, axis=0)


def in_one(arrays, axis):
    ends = [0]
    for a in arrays:
        ends.append(ends[-1] + a.size)
    so_far = over_copies(jnp.concatenate([a.ravel() for a in arrays]), axis)
    return tuple((so_far[b:e].reshape(a.shape) for a, b, e in zip(arrays, ends, ends[1:])))


def rows_first(arrays, axis, dims):
    turned = [jnp.moveaxis(a, dim, 0) for a, dim in zip(arrays, dims)]
    both = jnp.concatenate([t.reshape(len(t), -1) for t in turned], axis=1)
    filled, at, outs = (lax.all_gather(both, axis, axis=0, tiled=True), 0, [])
    for t, dim in zip(turned, dims):
        piece = filled[:, at : at + t[0].size].reshape(-1, *t.shape[1:])
        outs.append(jnp.moveaxis(piece, 0, dim))
        at += t[0].size
    return tuple(outs)


def laid_out(parts, dim):
    lengths = list(parts.shape[1:])
    lengths[dim] *= parts.shape[0]
    return jnp.moveaxis(parts, 0, dim).reshape(lengths)


def gather_in_order(array, axes, turns):
    parts = array
    for k in turns:
        parts = lax.all_gather(parts, axes[k])
    done = turns[::-1]
    back = [done.index(k) for k in range(len(axes))]
    parts = parts.transpose(*back, *range(len(axes), parts.ndim))
    return parts.reshape(-1, *array.shape)


def gather_axes(array, axes, turns, dim):
    return laid_out(gather_in_order(array, axes, turns), dim)


def gather_directly(array, axis, dim):
    parts = copy_for_each(array, axis)
    return laid_out(parts, dim)


def extended(array, sides, width):
    for axis, dim in sides:
        count, length = (lax.axis_size(axis), array.shape[dim])
        up = [(i, (i + 1) % count) for i in range(count - 1)]
        down = [(j, i) for i, j in up]
        last = lax.slice_in_dim(array, length - width, length, axis=dim)
        first = lax.slice_in_dim(array, 0, width, axis=dim)
        before = lax.ppermute(last, axis, up)
        after = lax.ppermute(first, axis, down)
        array = jnp.concatenate([before, array, after], axis=dim)
    return array


def collected_together(array, axis):
    leaves = jax.tree.leaves(array)
    turns = sorted(range(len(leaves)), key=lambda k: -leaves[k].size)
    width = (1, *leaves[turns[0]].shape)[-1]
    lines = [
        jnp.pad(leaves[k].reshape(-1), (0, -leaves[k].size % width)).reshape(-1, width)
        for k in turns
    ]
    both, at, found = (copy_for_each(jnp.concatenate(lines), axis), 0, {})
    for k, line in zip(turns, lines):
        piece = both[:, at : at + len(line)].reshape(len(both), -1)
        found[k] = piece[:, : leaves[k].size].reshape(-1, *leaves[k].shape)
        at += len(line)
    numbers = iter(range(len(leaves)))
    return jax.tree.map(lambda _: found[next(numbers)], array)


def folded_in_pairs(pieces, combine):
    while len(jax.tree.leaves(pieces)[0]) > 1:
        pieces = jax.vmap(combine)(
            *(jax.tree.map(lambda part: part[side::2], pieces) for side in (0, 1))
        )
    return jax.tree.map(lambda part: part[0], pieces)


def prefix(array, axis, combine, identity, reverse):
    count, place = (lax.axis_size(axis), lax.axis_index(axis))
    passed = jnp.arange(count) > place if reverse else jnp.arange(count) < place

    def kept(part, zero, own):
        part = jnp.where(
            passed.reshape(-1, *(1 for _ in own.shape)),
            part.astype(own.dtype),
            jnp.asarray(zero, own.dtype),
        )
        return part[::-1] if reverse else part

    pieces = collected_together(
        jax.tree.map(lambda part, kind: part.astype(kind), array, (jnp.bfloat16, jnp.bfloat16)),
        axis,
    )
    return folded_in_pairs(jax.tree.map(kept, pieces, identity, array), combine)


def modulated_norm(rows, gain, shift, scale):
    wide = rows.astype(jnp.float32)
    normed = (
        wide
        * lax.rsqrt(jnp.mean(wide * wide, axis=-1, keepdims=True) + EPS)
        * gain.astype(jnp.float32)
    )
    return (normed * (1.0 + scale) + shift).astype(jnp.bfloat16)


def project(rows, weights):
    outputs = [
        jnp.dot(rows, w, preferred_element_type=jnp.float32).astype(jnp.bfloat16) for w in weights
    ]
    return lax.optimization_barrier(outputs)


def centred_conv(padded, taps):
    wide = padded.astype(jnp.float32)
    weights = taps.astype(jnp.float32)
    length = padded.shape[0] - 2
    return jax.nn.silu(
        weights[0] * wide[:length] + weights[1] * wide[1 : length + 1] + weights[2] * wide[2:]
    )


def zero_pad(values):
    return jnp.pad(values, ((1, 1), (0, 0)))


def block_states(values, writes, step_size, decay_rate, block):
    length, heads, width = values.shape
    state = writes.shape[2]
    count = length // block
    log_decay = jnp.cumsum(-(step_size * decay_rate).reshape(count, block, heads), axis=1)
    scaled_values = (values * step_size[:, :, None]).reshape(count, block, heads, width)
    write_blocks = writes.reshape(count, block, heads, state)
    tail = jnp.exp(log_decay[:, -1:] - log_decay)
    block_sums = jnp.einsum(
        "kshn,ksh,kshp->khpn", write_blocks, tail, scaled_values, precision=lax.Precision.HIGHEST
    )
    block_decay = jnp.exp(log_decay[:, -1])

    def advance(carry, inputs):
        block_sum, decay = inputs
        return (carry * decay[:, None, None] + block_sum, carry)

    final, entering = lax.scan(
        advance, jnp.zeros((heads, width, state), jnp.float32), (block_sums, block_decay)
    )
    overall = jnp.exp(jnp.sum(log_decay[:, -1], axis=0))
    return (log_decay, scaled_values, entering, final, overall)


def block_outputs(reads, writes, log_decay, scaled_values, entering, start_state):
    count, block, heads = log_decay.shape
    state = reads.shape[2]
    read_blocks = reads.reshape(count, block, heads, state)
    write_blocks = writes.reshape(count, block, heads, state)
    starts = jnp.cumsum(log_decay[:, -1], axis=0) - log_decay[:, -1]
    entering_all = entering + jnp.exp(starts)[:, :, None, None] * start_state[None]
    forward_mask = jnp.tril(jnp.ones((block, block), bool))[None, :, :, None]
    spans = log_decay[:, :, None, :] - log_decay[:, None, :, :]
    weights = jnp.where(forward_mask, jnp.exp(jnp.where(forward_mask, spans, 0.0)), 0.0)
    intersection = jnp.einsum(
        "kqhn,kshn->kqsh", read_blocks, write_blocks, precision=lax.Precision.HIGHEST
    )
    within = jnp.einsum(
        "kqsh,kshp->kqhp", intersection * weights, scaled_values, precision=lax.Precision.HIGHEST
    )
    carried = (
        jnp.einsum("kqhn,khpn->kqhp", read_blocks, entering_all, precision=lax.Precision.HIGHEST)
        * jnp.exp(log_decay)[..., None]
    )
    return (within + carried).reshape(count * block, heads, -1)


def chain(earlier, later):
    return (earlier[0] * later[0], earlier[1] * later[0][:, None, None] + later[1])


def per_device(
    latent,
    context,
    cond,
    cond_ctx,
    mod_shift_w,
    mod_scale_w,
    mod_gate_w,
    norm_gain,
    proj_z,
    proj_x,
    proj_b,
    proj_c,
    proj_dt,
    conv_x,
    conv_b,
    conv_c,
    dt_bias,
    decay_log,
    head_gain,
    proj_out,
):
    heads = proj_x.shape[1] // HEAD_DIM
    state = proj_b.shape[1] // heads
    width_x = heads * HEAD_DIM
    width_b = heads * state
    act = jax.nn.silu(cond.astype(jnp.float32)).astype(jnp.bfloat16)
    act_ctx = jax.nn.silu(cond_ctx.astype(jnp.float32)).astype(jnp.bfloat16)
    stacked = jnp.stack([act, act_ctx])
    shift_part = jnp.dot(stacked, mod_shift_w, preferred_element_type=jnp.float32)
    scale_part = jnp.dot(stacked, mod_scale_w, preferred_element_type=jnp.float32)
    gate_part = jnp.dot(act[None], mod_gate_w, preferred_element_type=jnp.float32)
    shift_sum, scale_sum, gate_sum = in_one((shift_part, scale_part, gate_part), "sp")
    shifts, scales, gates = rows_first((shift_sum, scale_sum, gate_sum), TP, (1, 1, 1))
    normed_rows = modulated_norm(latent, norm_gain, shifts[0], scales[0])
    normed_ctx = modulated_norm(context, norm_gain, shifts[1], scales[1])
    dt_weight = lax.dynamic_slice_in_dim(proj_dt, lax.axis_index(TP) * (2 * heads), 2 * heads, 1)
    joined = jnp.concatenate(
        project(
            gather_axes(normed_rows, TP, (1, 0, 2), 0), (proj_x, proj_b, proj_c, proj_z, dt_weight)
        ),
        axis=1,
    )
    ctx_joined = gather_directly(
        jnp.concatenate(project(normed_ctx, (proj_x, proj_b, dt_weight)), axis=1), "sp", 0
    )
    length = joined.shape[0]
    ctx_length = ctx_joined.shape[0]
    conv_end = width_x + 2 * width_b
    padded = extended(joined[:, :conv_end], (("sp", 0),), 1)
    convolved = centred_conv(padded, jnp.concatenate([conv_x, conv_b, conv_c], axis=1))
    values = convolved[:, :width_x].reshape(length, heads, HEAD_DIM)
    writes = convolved[:, width_x : width_x + width_b].reshape(length, heads, state)
    reads = convolved[:, width_x + width_b :].reshape(length, heads, state)
    z_in = joined[:, conv_end : conv_end + width_x]
    step_size = jax.nn.softplus(
        joined[:, conv_end + width_x :].astype(jnp.float32) + dt_bias
    ).reshape(length, heads, 2)
    decay_rate = jnp.exp(decay_log).reshape(heads, 2)
    ctx_conv = centred_conv(
        zero_pad(ctx_joined[:, : width_x + width_b]), jnp.concatenate([conv_x, conv_b], axis=1)
    )
    values_ctx = ctx_conv[:, :width_x].reshape(ctx_length, heads, HEAD_DIM)
    writes_ctx = ctx_conv[:, width_x:].reshape(ctx_length, heads, state)
    step_ctx = jax.nn.softplus(
        ctx_joined[:, width_x + width_b :].astype(jnp.float32) + dt_bias
    ).reshape(ctx_length, heads, 2)
    ctx_f = block_states(values_ctx, writes_ctx, step_ctx[:, :, 0], decay_rate[:, 0], BLOCK)[3]
    ctx_b = block_states(
        jnp.flip(values_ctx, 0),
        jnp.flip(writes_ctx, 0),
        jnp.flip(step_ctx[:, :, 1], 0),
        decay_rate[:, 1],
        BLOCK,
    )[3]
    log_f, scaled_f, enter_f, final_f, overall_f = block_states(
        values, writes, step_size[:, :, 0], decay_rate[:, 0], BLOCK
    )
    reads_back = jnp.flip(reads, 0)
    writes_back = jnp.flip(writes, 0)
    log_b, scaled_b, enter_b, final_b, overall_b = block_states(
        jnp.flip(values, 0), writes_back, jnp.flip(step_size[:, :, 1], 0), decay_rate[:, 1], BLOCK
    )
    identity = (jnp.ones((heads,), jnp.float32), jnp.zeros((heads, HEAD_DIM, state), jnp.float32))
    before = prefix((overall_f, final_f), "sp", chain, identity, False)
    after = prefix((overall_b, final_b), "sp", chain, identity, True)
    start_f = before[1] + before[0][:, None, None] * ctx_f
    start_b = after[1] + after[0][:, None, None] * ctx_b
    out_f = block_outputs(reads, writes, log_f, scaled_f, enter_f, start_f)
    out_b = block_outputs(reads_back, writes_back, log_b, scaled_b, enter_b, start_b)
    summed = out_f + jnp.flip(out_b, 0)
    gated = summed * jax.nn.silu(z_in.astype(jnp.float32)).reshape(length, heads, HEAD_DIM)
    gated = gated * lax.rsqrt(jnp.mean(gated * gated, axis=-1, keepdims=True) + EPS)
    gated = gated * head_gain.astype(jnp.float32).reshape(heads, HEAD_DIM)
    mixed_heads = gated.reshape(length, width_x).astype(jnp.bfloat16)
    update_cols = jnp.dot(
        gather_directly(mixed_heads, TP, 1), proj_out, preferred_element_type=jnp.float32
    )
    update_rows = lax.all_to_all(
        update_cols.astype(jnp.bfloat16), TP, split_axis=0, concat_axis=1, tiled=True
    )
    update = lax.optimization_barrier(update_rows).astype(jnp.float32)
    return (latent.astype(jnp.float32) + gates[0] * update).astype(jnp.bfloat16)


def solution(mesh):
    torus = Mesh(mesh.devices.reshape(mesh.shape["sp"], 8, 4, 2), ("sp", "tp_0", "tp_1", "tp_2"))
    in_specs = (
        P(SP_TP, None),
        P("sp", None),
        P("sp"),
        P("sp"),
        P("sp", TP),
        P("sp", TP),
        P("sp", TP),
        P(),
        P(None, TP),
        P(None, TP),
        P(None, TP),
        P(None, TP),
        P(),
        P(None, TP),
        P(None, TP),
        P(None, TP),
        P(TP),
        P(TP),
        P(TP),
        P(None, TP),
    )
    out_specs = P(SP_TP, None)
    return jax.shard_map(
        per_device, mesh=torus, in_specs=in_specs, out_specs=out_specs, check_vma=False
    )
```

profile of v0, /device:TPU:1, one launch (start us, length us, event | category | flops | bytes accessed | tf_op | source)
XLA Modules:
  0.0 349.2 jit_solution(14793010596654046668)
XLA Ops:
  8.1 0.9 fusion.73
  9.0 0.9 fusion.74
  11.5 19.4 %all-to-all-start = ((f32[16,1,320]{2,1,0:T(1,128)}), f32[16,1,320]{2,1,0:T(1,128)S(1)}, u32[]{:S(2)}, u32[]{:S(2)}) async-start(f32[16,1,320]{2,1,0:T(1,128)} %broadcast_in_dim.114), calls=%async_computation | async-start | bytes 49152 | tf_op jit(solution)/shard_map/all_to_all | solution.py:18
  31.0 0.9 fusion.26
  32.6 9.8 %all-to-all-done = f32[16,1,320]{2,1,0:T(1,128)S(1)} async-done(((f32[16,1,320]{2,1,0:T(1,128)}), f32[16,1,320]{2,1,0:T(1,128)S(1)}, u32[]{:S(2)}, u32[]{:S(2)}) %all-to-all-start) | async-done | bytes 20512 | tf_op jit(solution)/shard_map/all_to_all | solution.py:18
  42.6 42.2 %all-gather.3 = f32[64,64,5]{1,2,0:T(8,128)S(1)} all-gather(f32[1,64,5]{1,2,0:T(8,128)S(1)} %maximum_bitcast_fusion), channel_id=1, replica_groups=mesh['sp'=16,'tp_0'=8,'tp_1'=4,'tp_2'=2] {'tp_0','tp_1','tp_2'}, dimensions={0}, use_global_device_ids=true | all-gather | bytes 83200 | tf_op jit(solution)/shard_map/all_gather | solution.py:37
  85.9 9.8 %all-gather.4 = bf16[4,4,4096]{2,1,0:T(4,128)(2,1)} all-gather(bf16[1,4,4096]{2,1,0:T(4,128)(2,1)S(1)} %fusion.43), channel_id=2, replica_groups=mesh['sp'=16,'tp_0'=8,'tp_1'=4,'tp_2'=2] {'tp_1'}, dimensions={0}, use_global_device_ids=true | all-gather | bytes 163840 | tf_op jit(solution)/shard_map/all_gather | solution.py:54
  95.8 1.1 fusion.14
  96.9 30.4 %all-gather.8.cloned.1.call-done = bf16[32,4,4096]{2,1,0:T(4,128)(2,1)} async-done(((bf16[4,4,4096]{2,1,0:T(4,128)(2,1)}), bf16[32,4,4096]{2,1,0:T(4,128)(2,1)}) %all-gather.8.cloned.1.call-update) | async-done | bytes 1048592 | tf_op jit(solution)/shard_map/all_gather | solution.py:54
  129.7 12.8 %all-to-all-start.2 = ((bf16[16,16,194]{2,1,0:T(8,128)(2,1)}), bf16[16,16,194]{2,1,0:T(8,128)(2,1)S(1)}, u32[]{:S(2)}, u32[]{:S(2)}) async-start(bf16[16,16,194]{2,1,0:T(8,128)(2,1)} %broadcast_in_dim.121), calls=%async_computation.2 | async-start | bytes 262144 | tf_op jit(solution)/shard_map/all_to_all | solution.py:18
  145.1 9.5 %all-to-all-done.2 = bf16[16,16,194]{2,1,0:T(8,128)(2,1)S(1)} async-done(((bf16[16,16,194]{2,1,0:T(8,128)(2,1)}), bf16[16,16,194]{2,1,0:T(8,128)(2,1)S(1)}, u32[]{:S(2)}, u32[]{:S(2)}) %all-to-all-start.2) | async-done | bytes 99360 | tf_op jit(solution)/shard_map/all_to_all | solution.py:18
  156.3 4.7 %all-gather.10.cloned.1.call-done = bf16[16,4,4,4096]{3,2,1,0:T(4,128)(2,1)} async-done(((bf16[8,4,4,4096]{3,2,1,0:T(4,128)(2,1)}), bf16[16,4,4,4096]{3,2,1,0:T(4,128)(2,1)}) %all-gather.10.cloned.1.call-update) | async-done | bytes 2097168 | tf_op jit(solution)/shard_map/all_gather | solution.py:54
  161.0 2.7 copy.227
  163.8 3.0 copy.178
  166.7 2.5 reshape_reshape.2
  169.3 2.4 convolution_convert_fusion.4
  172.9 1.3 convolution_convert_fusion.8
  175.3 1.4 convolution_convert_fusion.3
  182.5 1.3 collective-permute-start.1
  183.8 4.0 %collective-permute-start = (bf16[1,320]{1,0:T(2,128)(2,1)S(1)}, bf16[1,320]{1,0:T(2,128)(2,1)S(1)}, u32[]{:S(2)}, u32[]{:S(2)}) collective-permute-start(bf16[1,320]{1,0:T(2,128)(2,1)S(1)} %get-tuple-element.374), channel_id=1, source_target_pairs={{0,64},{64,128},{128,192},{192,256},{256,320},{320,384},{384,448},... | collective-permute-start | bytes 1928 | tf_op jit(solution)/shard_map/ppermute | solution.py:77
  189.3 2.3 while.51
  193.0 2.5 while.49
  197.1 2.4 while.50
  200.2 10.3 %all-to-all-start.3 = ((bf16[16,65,128]{2,1,0:T(8,128)(2,1)}), bf16[16,65,128]{2,1,0:T(8,128)(2,1)S(1)}, u32[]{:S(2)}, u32[]{:S(2)}) async-start(bf16[16,65,128]{2,1,0:T(8,128)(2,1)} %broadcast_in_dim.123), calls=%async_computation.3 | async-start | bytes 589824 | tf_op jit(solution)/shard_map/all_to_all | solution.py:18
  210.9 2.4 while.48
  213.7 10.9 %all-to-all-done.3 = bf16[16,65,128]{2,1,0:T(8,128)(2,1)S(1)} async-done(((bf16[16,65,128]{2,1,0:T(8,128)(2,1)}), bf16[16,65,128]{2,1,0:T(8,128)(2,1)S(1)}, u32[]{:S(2)}, u32[]{:S(2)}) %all-to-all-start.3) | async-done | bytes 266272 | tf_op jit(solution)/shard_map/all_to_all | solution.py:18
  225.4 11.4 %all-to-all-start.1 = ((bf16[16,65,128]{2,1,0:T(8,128)(2,1)}), bf16[16,65,128]{2,1,0:T(8,128)(2,1)S(1)}, u32[]{:S(2)}, u32[]{:S(2)}) async-start(bf16[16,65,128]{2,1,0:T(8,128)(2,1)} %broadcast_in_dim.118), calls=%async_computation.1 | async-start | bytes 589824 | tf_op jit(solution)/shard_map/all_to_all | solution.py:18
  238.3 12.5 %all-to-all-done.1 = bf16[16,65,128]{2,1,0:T(8,128)(2,1)S(1)} async-done(((bf16[16,65,128]{2,1,0:T(8,128)(2,1)}), bf16[16,65,128]{2,1,0:T(8,128)(2,1)S(1)}, u32[]{:S(2)}, u32[]{:S(2)}) %all-to-all-start.1) | async-done | bytes 266272 | tf_op jit(solution)/shard_map/all_to_all | solution.py:18
  258.2 65.7 %all_to_all.45 = bf16[64,256,64]{1,2,0:T(8,128)(2,1)S(1)} all-to-all(bf16[64,256,64]{1,2,0:T(8,128)(2,1)S(1)} %broadcast_in_dim.124), channel_id=1, replica_groups=mesh['sp'=16,'tp_0'=8,'tp_1'=4,'tp_2'=2] {'tp_0','tp_1','tp_2'}, dimensions={0} | all-to-all | bytes 4194304 | tf_op jit(solution)/shard_map/all_to_all | solution.py:18
  325.2 7.0 %all-to-all-start.5 = ((bf16[64,2,128]{2,1,0:T(2,128)(2,1)}), bf16[64,2,128]{2,1,0:T(2,128)(2,1)S(1)}, u32[]{:S(2)}, u32[]{:S(2)}) async-start(bf16[64,2,128]{2,1,0:T(2,128)(2,1)} %reshape.755), calls=%async_computation.5 | async-start | bytes 65536 | tf_op jit(solution)/shard_map/all_to_all | solution.py:306
  332.1 0.9 slice.368
  333.1 8.4 %all-to-all-done.5 = bf16[64,2,128]{2,1,0:T(2,128)(2,1)S(1)} async-done(((bf16[64,2,128]{2,1,0:T(2,128)(2,1)}), bf16[64,2,128]{2,1,0:T(2,128)(2,1)S(1)}, u32[]{:S(2)}, u32[]{:S(2)}) %all-to-all-start.5) | async-done | bytes 32800 | tf_op jit(solution)/shard_map/all_to_all | solution.py:306
  (253 shorter events, 43.0 us)
Async XLA Ops:
  6.5 122.1 %copy-start = (bf16[4096,128]{1,0:T(8,128)(2,1)S(1)}, bf16[4096,128]{1,0:T(8,128)(2,1)}, u32[]{:S(2)}) copy-start(bf16[4096,128]{1,0:T(8,128)(2,1)} %param.38) | copy-start | bytes 3145732
  6.5 121.3 %copy-start.3 = (bf16[16,4096]{1,0:T(8,128)(2,1)S(1)}, bf16[16,4096]{1,0:T(8,128)(2,1)}, u32[]{:S(2)}) copy-start(bf16[16,4096]{1,0:T(8,128)(2,1)} %param.29) | copy-start | bytes 393220
  6.5 121.3 %copy-start.26 = (f32[2]{0:T(128)S(1)}, f32[2]{0:T(128)}, u32[]{:S(2)}) copy-start(f32[2]{0:T(128)} %param.45) | copy-start | bytes 28
  6.5 121.3 %copy-start.1 = (bf16[4096,128]{1,0:T(8,128)(2,1)S(1)}, bf16[4096,128]{1,0:T(8,128)(2,1)}, u32[]{:S(2)}) copy-start(bf16[4096,128]{1,0:T(8,128)(2,1)} %param.40) | copy-start | bytes 3145732
  11.5 30.8 %all-to-all-start = ((f32[16,1,320]{2,1,0:T(1,128)}), f32[16,1,320]{2,1,0:T(1,128)S(1)}, u32[]{:S(2)}, u32[]{:S(2)}) async-start(f32[16,1,320]{2,1,0:T(1,128)} %broadcast_in_dim.114), calls=%async_computation | async-start | bytes 49152 | tf_op jit(solution)/shard_map/all_to_all | solution.py:18
  30.9 96.4 %all-gather.8.cloned.1.call-start = ((), (), s32[]{:S(2)}) async-start(), calls=%async_computation.6 | async-start | bytes 1179648 | tf_op jit(solution)/shard_map/all_gather | solution.py:54
  32.6 95.7 %copy-start.4 = (bf16[4096,64]{0,1:T(8,128)(2,1)S(1)}, bf16[4096,64]{0,1:T(8,128)(2,1)}, u32[]{:S(2)}) copy-start(bf16[4096,64]{0,1:T(8,128)(2,1)} %param.37) | copy-start | bytes 1572868
  84.9 44.0 %copy-start.11 = (f32[4096,5]{0,1:T(8,128)}, f32[4096,5]{0,1:T(8,128)S(1)}, u32[]{:S(2)}) copy-start(f32[4096,5]{0,1:T(8,128)S(1)} %reshape.728) | copy-start | bytes 245764
  95.8 65.2 %all-gather.10.cloned.1.call-start = ((), (), s32[]{:S(2)}) async-start(), calls=%async_computation.7 | async-start | bytes 3145728 | tf_op jit(solution)/shard_map/all_gather | solution.py:54
  127.3 15.8 %copy-start.27 = (bf16[64]{0:T(256)(128)(2,1)S(1)}, bf16[64]{0:T(256)(128)(2,1)}, u32[]{:S(2)}) copy-start(bf16[64]{0:T(256)(128)(2,1)} %param.46) | copy-start | bytes 388
  127.3 16.4 %copy-start.19 = (bf16[3,128]{1,0:T(4,128)(2,1)S(1)}, bf16[3,128]{1,0:T(4,128)(2,1)}, u32[]{:S(2)}) copy-start(bf16[3,128]{1,0:T(4,128)(2,1)} %param.42) | copy-start | bytes 2308
  127.3 16.4 %copy-start.20 = (bf16[3,64]{1,0:T(4,128)(2,1)S(1)}, bf16[3,64]{1,0:T(4,128)(2,1)}, u32[]{:S(2)}) copy-start(bf16[3,64]{1,0:T(4,128)(2,1)} %param.41) | copy-start | bytes 1156
  127.3 16.4 %copy-start.21 = (bf16[3,128]{1,0:T(4,128)(2,1)S(1)}, bf16[3,128]{1,0:T(4,128)(2,1)}, u32[]{:S(2)}) copy-start(bf16[3,128]{1,0:T(4,128)(2,1)} %param.43) | copy-start | bytes 2308
  129.7 24.8 %all-to-all-start.2 = ((bf16[16,16,194]{2,1,0:T(8,128)(2,1)}), bf16[16,16,194]{2,1,0:T(8,128)(2,1)S(1)}, u32[]{:S(2)}, u32[]{:S(2)}) async-start(bf16[16,16,194]{2,1,0:T(8,128)(2,1)} %broadcast_in_dim.121), calls=%async_computation.2 | async-start | bytes 262144 | tf_op jit(solution)/shard_map/all_to_all | solution.py:18
  155.5 8.3 %copy-start.6 = (f32[256,192]{1,0:T(8,128)}, f32[256,192]{1,0:T(8,128)S(1)}, u32[]{:S(2)}) copy-start(f32[256,192]{1,0:T(8,128)S(1)} %divide_multiply_fusion.1) | copy-start | bytes 589828
  176.7 5.6 %copy-start.14 = (bf16[256,64]{0,1:T(8,128)(2,1)S(1)}, bf16[256,64]{0,1:T(8,128)(2,1)}, u32[]{:S(2)}) copy-start(bf16[256,64]{0,1:T(8,128)(2,1)} %convolution_convert_fusion.4) | copy-start | bytes 98308
  176.7 11.9 %copy-start.7 = (f32[256,192]{1,0:T(8,128)S(1)}, f32[256,192]{1,0:T(8,128)}, u32[]{:S(2)}) copy-start(f32[256,192]{1,0:T(8,128)} %copy-done.6) | copy-start | bytes 589828
  176.7 12.4 %copy-start.8 = (f32[256,128]{1,0:T(8,128)S(1)}, f32[256,128]{1,0:T(8,128)}, u32[]{:S(2)}) copy-start(f32[256,128]{1,0:T(8,128)} %reverse.23) | copy-start | bytes 393220
  182.3 13.6 %copy-start.15 = (f32[320]{0:T(512)S(1)}, f32[320]{0:T(512)}, u32[]{:S(2)}) copy-start(f32[320]{0:T(512)} %get-tuple-element.327) | copy-start | bytes 3844
  182.3 13.6 %copy-start.16 = (f32[320]{0:T(512)S(1)}, f32[320]{0:T(512)}, u32[]{:S(2)}) copy-start(f32[320]{0:T(512)} %get-tuple-element.328) | copy-start | bytes 3844
  182.3 13.6 %copy-start.17 = (f32[320]{0:T(512)S(1)}, f32[320]{0:T(512)}, u32[]{:S(2)}) copy-start(f32[320]{0:T(512)} %get-tuple-element.329) | copy-start | bytes 3844
  182.5 13.2 %collective-permute-start.1 = (bf16[1,320]{1,0:T(2,128)(2,1)S(1)}, bf16[1,320]{1,0:T(2,128)(2,1)S(1)}, u32[]{:S(2)}, u32[]{:S(2)}) collective-permute-start(bf16[1,320]{1,0:T(2,128)(2,1)S(1)} %get-tuple-element.375), channel_id=1, source_target_pairs={{64,0},{128,64},{192,128},{256,192},{320,256},{384,320},{448,384},... | collective-permute-start | bytes 1928 | tf_op jit(solution)/shard_map/ppermute | solution.py:78
  183.8 11.9 %collective-permute-start = (bf16[1,320]{1,0:T(2,128)(2,1)S(1)}, bf16[1,320]{1,0:T(2,128)(2,1)S(1)}, u32[]{:S(2)}, u32[]{:S(2)}) collective-permute-start(bf16[1,320]{1,0:T(2,128)(2,1)S(1)} %get-tuple-element.374), channel_id=1, source_target_pairs={{0,64},{64,128},{128,192},{192,256},{256,320},{320,384},{384,448},... | collective-permute-start | bytes 1928 | tf_op jit(solution)/shard_map/ppermute | solution.py:77
  200.2 24.4 %all-to-all-start.3 = ((bf16[16,65,128]{2,1,0:T(8,128)(2,1)}), bf16[16,65,128]{2,1,0:T(8,128)(2,1)S(1)}, u32[]{:S(2)}, u32[]{:S(2)}) async-start(bf16[16,65,128]{2,1,0:T(8,128)(2,1)} %broadcast_in_dim.123), calls=%async_computation.3 | async-start | bytes 589824 | tf_op jit(solution)/shard_map/all_to_all | solution.py:18
  210.5 40.7 %copy-start.24 = (pred[16]{0:T(512)(128)(4,1)S(1)}, pred[16]{0:T(512)(128)(4,1)}, u32[]{:S(2)}) copy-start(pred[16]{0:T(512)(128)(4,1)} %iota_compare_fusion.3) | copy-start | bytes 52
  225.4 25.5 %all-to-all-start.1 = ((bf16[16,65,128]{2,1,0:T(8,128)(2,1)}), bf16[16,65,128]{2,1,0:T(8,128)(2,1)S(1)}, u32[]{:S(2)}, u32[]{:S(2)}) async-start(bf16[16,65,128]{2,1,0:T(8,128)(2,1)} %broadcast_in_dim.118), calls=%async_computation.1 | async-start | bytes 589824 | tf_op jit(solution)/shard_map/all_to_all | solution.py:18
  237.9 17.4 %copy-start.25 = (pred[16]{0:T(512)(128)(4,1)S(1)}, pred[16]{0:T(512)(128)(4,1)}, u32[]{:S(2)}) copy-start(pred[16]{0:T(512)(128)(4,1)} %iota_compare_fusion.4) | copy-start | bytes 52
  252.1 5.6 %copy-start.13 = (bf16[256,64]{0,1:T(8,128)(2,1)S(1)}, bf16[256,64]{0,1:T(8,128)(2,1)}, u32[]{:S(2)}) copy-start(bf16[256,64]{0,1:T(8,128)(2,1)} %convolution_convert_fusion.3) | copy-start | bytes 98308
  252.1 5.7 %copy-start.22 = (f32[64]{0:T(128)S(1)}, f32[64]{0:T(128)}, u32[]{:S(2)}) copy-start(f32[64]{0:T(128)} %convert_element_type.163) | copy-start | bytes 772
  258.2 65.7 %copy-start.10 = (bf16[4096,64]{0,1:T(8,128)(2,1)S(1)}, bf16[4096,64]{0,1:T(8,128)(2,1)}, u32[]{:S(2)}) copy-start(bf16[4096,64]{0,1:T(8,128)(2,1)} %param.47) | copy-start | bytes 1572868
  323.9 17.8 %copy-start.12 = (bf16[4,4096]{1,0:T(4,128)(2,1)S(1)}, bf16[4,4096]{1,0:T(4,128)(2,1)}, u32[]{:S(2)}) copy-start(bf16[4,4096]{1,0:T(4,128)(2,1)} %param.28) | copy-start | bytes 98308
  325.2 16.3 %all-to-all-start.5 = ((bf16[64,2,128]{2,1,0:T(2,128)(2,1)}), bf16[64,2,128]{2,1,0:T(2,128)(2,1)S(1)}, u32[]{:S(2)}, u32[]{:S(2)}) async-start(bf16[64,2,128]{2,1,0:T(2,128)(2,1)} %reshape.755), calls=%async_computation.5 | async-start | bytes 65536 | tf_op jit(solution)/shard_map/all_to_all | solution.py:306
  (5 other events, 6.4 us)
Sparse Core Ops, SparseCore 0:
  95.9 31.3 all-gather.7
  130.0 31.0 all-gather.9
where the time goes:
time: 351 us; the launch traced here: 349 us
  blocking collectives  118 us (34%)
  waiting for transfers between devices  86.3 us (25%)
  starting transfers between devices  66.2 us (19%)
  local copies, waits for them, and re-layouts  25.1 us (7%)
  other arithmetic  21.7 us (6%)
  between operations  18 us (5%)
  matrix products  14 us (4%)
    all_to_all x1, blocking collectives, copy_for_each(): return lax.all_to_all(copies, axis, split_axis=0, concat_axis=0, tiled=True)  65.7 us
    all_to_all x4, starting transfers between devices, copy_for_each(): return lax.all_to_all(copies, axis, split_axis=0, concat_axis=0, tiled=True)  53.8 us
    all_to_all x4, waiting for transfers between devices, copy_for_each(): return lax.all_to_all(copies, axis, split_axis=0, concat_axis=0, tiled=True)  42.7 us
    all_gather x1, blocking collectives, rows_first(): filled, at, outs = (lax.all_gather(both, axis, axis=0, tiled=True), 0, [])  42.2 us
    all_gather x2, waiting for transfers between devices, gather_in_order(): parts = lax.all_gather(parts, axes[k])  35.1 us
    all_gather x1, blocking collectives, gather_in_order(): parts = lax.all_gather(parts, axes[k])  9.85 us
    all_to_all x1, waiting for transfers between devices, per_device(): lax.all_to_all(update_cols.astype(jnp.bfloat16), TP, split_axis=0, concat...  8.4 us
    dot_general x8, matrix products, project(): jnp.dot(rows, w, preferred_element_type=jnp.float32).astype(jnp.bfloat16)  7.6 us
  transfers between devices with their start and end apart: 9, of which 7 were waited for; matrix products, arithmetic and copies ran while one was open for 6% of the time, Pallas kernels for 0%

commit v1 on v0

v1 whole, which is shorter than its diff:
```python
import functools

import jax
import jax.numpy as jnp
from jax import lax
from jax.experimental import pallas as pl
from jax.experimental.pallas import tpu as pltpu
from jax.sharding import Mesh
from jax.sharding import PartitionSpec as P

TP = ("tp_0", "tp_1", "tp_2")
SP_TP = ("sp", "tp_0", "tp_1", "tp_2")
EPS = 1e-06
MESH_ID = pl.DeviceIdType.MESH
F32 = jnp.float32
BF16 = jnp.bfloat16
HI = lax.Precision.HIGHEST


def iota(shape, dim):
    return lax.broadcasted_iota(jnp.int32, shape, dim)


def silu(v):
    return v * (1.0 / (1.0 + jnp.exp(-v)))


def softplus(v):
    return jnp.maximum(v, 0.0) + jnp.log1p(jnp.exp(-jnp.abs(v)))


def bdot(a, b, dims=(((1,), (0,)), ((), ()))):
    return lax.dot_general(a.astype(BF16), b.astype(BF16), dims, preferred_element_type=F32)


def hdot(a, b):
    return jnp.dot(a, b, precision=HI, preferred_element_type=F32)


def kernel(
    sizes,
    lat_ref, ctx_ref, cond_ref, condc_ref, wsh_ref, wsc_ref, wga_ref, gain_ref,
    pz_ref, px_ref, pb_ref, pc_ref, pdt_ref, cx_ref, cb_ref, cc_ref, dtb_ref, dlog_ref, hg_ref, po_ref,
    out_ref,
    wcat, wx, wz, wo_own, wo_part, wo, latbuf, pbuf, psend, mpair, mpair_r, mbuf, sbuf, acc, accs,
    cbuf, ebuf, esend, lbuf, snd, rst, osend, orecv, obuf, ubuf, rbuf, cst,
    wsem, wosem, worsem, pss, prs, mps, mpr, m1s, m1r, m2s, m2r, lgs, lgr, ld_s, ldr,
    css, csr, es, er, ls_, lr_, sts, str_, ops, opr, ogs, ogr, us, ur,
):
    Z, Y, X = sizes
    NC = Y * X
    HC = NC // 2
    D = lat_ref.shape[1]
    HD = D // 2
    T = NC * 8
    TH = T // 2
    CZ = ctx_ref.shape[0]
    CT = CZ * Z
    z = lax.axis_index("sp")
    y = lax.axis_index("tp_0")
    x = lax.axis_index("tp_1")
    c = lax.axis_index("tp_2")
    chip = y * X + x
    head = chip * 2 + c
    first_core = c == 0

    def remote(src, dst, ssem, rsem, dev):
        return pltpu.make_async_remote_copy(
            src_ref=src, dst_ref=dst, send_sem=ssem, recv_sem=rsem, device_id=dev, device_id_type=MESH_ID
        )

    def drain(ref, sem):
        pltpu.make_async_copy(ref, ref, sem).wait()

    partner = {"tp_2": 1 - c}

    loads = [
        pltpu.make_async_copy(px_ref, wx, wsem.at[0]),
        pltpu.make_async_copy(pz_ref, wz, wsem.at[1]),
        pltpu.make_async_copy(pb_ref, wcat.at[:, 128:256], wsem.at[2]),
        pltpu.make_async_copy(pc_ref, wcat.at[:, 256:384], wsem.at[3]),
        pltpu.make_async_copy(pdt_ref, wcat.at[:, 384:512], wsem.at[4]),
        pltpu.make_async_copy(po_ref, wo_own, wsem.at[5]),
    ]
    for load in loads:
        load.start()

    bar = pltpu.get_barrier_semaphore()

    def greet_z(i, carry):
        pl.semaphore_signal(bar, inc=1, device_id={"sp": lax.rem(z + i, Z)}, device_id_type=MESH_ID)
        return carry

    def greet_plane(i, carry):
        j = lax.rem(chip * 2 + c + i, NC * 2)
        k = j // 2
        pl.semaphore_signal(
            bar, inc=1, device_id={"tp_0": k // X, "tp_1": lax.rem(k, X), "tp_2": lax.rem(j, 2)},
            device_id_type=MESH_ID,
        )
        return carry

    lax.fori_loop(1, Z, greet_z, 0)
    lax.fori_loop(1, NC * 2, greet_plane, 0)

    row8 = iota((8, cond_ref.shape[1]), 0)
    both = jnp.where(row8 == 0, cond_ref[...].astype(F32), jnp.where(row8 == 1, condc_ref[...].astype(F32), 0.0))
    act = silu(both).astype(BF16)

    def wide(part):
        zero = jnp.zeros_like(part)
        return jnp.where(first_core, jnp.concatenate([part, zero], 1), jnp.concatenate([zero, part], 1))

    psh = wide(jnp.dot(act, wsh_ref[...], preferred_element_type=F32))
    psc = wide(jnp.dot(act, wsc_ref[...], preferred_element_type=F32))
    pga = wide(jnp.dot(act, wga_ref[...], preferred_element_type=F32))
    mpair[...] = jnp.concatenate([psh[0:1], psc[0:1], psh[1:2], psc[1:2], pga[0:1]], 0)

    def sq_ctx(k, tot):
        v = ctx_ref[:, pl.ds(pl.multiple_of(k * 128, 128), 128)].astype(F32)
        return tot + v * v

    tot = lax.fori_loop(0, NC, sq_ctx, jnp.zeros((CZ, 128), F32))
    r_ctx = lax.rsqrt(jnp.sum(tot, axis=1, keepdims=True) / D + EPS)

    psend[...] = lat_ref[:, pl.ds(pl.multiple_of((1 - c) * HD, 128), HD)]

    for load in loads[:2]:
        load.wait()
    RB = min(512, D)

    def join_w(i, carry):
        rows = pl.ds(pl.multiple_of(i * RB, RB), RB)
        wcat[rows, 0:128] = jnp.concatenate([wx[rows, :], wz[rows, :]], 1)
        return carry

    lax.fori_loop(0, D // RB, join_w, 0)
    for load in loads[2:]:
        load.wait()

    pl.semaphore_wait(bar, Z - 1 + NC * 2 - 1)

    lp = remote(psend, pbuf, pss, prs, partner)
    lp.start()
    mp = remote(mpair, mpair_r, mps, mpr, partner)
    mp.start()
    wocopy = remote(wo_own, wo_part, wosem, worsem, partner)

    def gather_send(buf, ssem, rsem, slot, dev):
        remote(buf.at[slot], buf.at[slot], ssem, rsem.at[slot], dev).start()

    def gather_wait(buf, ssem, rsem, slot):
        remote(buf.at[slot], buf.at[slot], ssem, rsem.at[slot], partner).wait_recv()

    def along_x(buf, ssem, rsem, slot):
        for d in (1, 3, 2) if X == 4 else range(1, X):
            gather_send(buf, ssem, rsem, slot, {"tp_1": lax.rem(x + d, X)})

    def y_step(i):
        k = i // 2 + 1
        odd = lax.rem(i, 2)
        return lax.rem(y + k * (1 - odd) + (Y - k) * odd, Y)

    def gather_open(buf, ssem, rsem):
        along_x(buf, ssem, rsem, chip)

        def go(i, carry):
            gather_send(buf, ssem, rsem, chip, {"tp_0": y_step(i)})
            return carry

        lax.fori_loop(0, Y - 1, go, 0)

    def gather_relay(buf, ssem, rsem, extra):
        def go(i, carry):
            slot = y_step(i) * X + x
            gather_wait(buf, ssem, rsem, slot)
            along_x(buf, ssem, rsem, slot)
            extra(slot)
            return carry

        lax.fori_loop(0, Y - 1, go, 0)

    def gather_close(buf, ssem, rsem, extra):
        def go(i, carry):
            yy = lax.rem(y + i // (X - 1), Y)
            xx = lax.rem(x + 1 + lax.rem(i, X - 1), X)
            slot = yy * X + xx
            gather_wait(buf, ssem, rsem, slot)
            extra(slot)
            return carry

        lax.fori_loop(0, Y * (X - 1), go, 0)

    def gather_drain(buf, ssem):
        n = Y - 1 + (X - 1) * Y
        drain(buf.at[pl.ds(0, n)], ssem)

    mine = latbuf.at[c]
    other = latbuf.at[1 - c]

    def to_partner(slot):
        remote(mine.at[slot], mine.at[slot], ld_s, ldr.at[slot], partner).start()

    lp.wait_recv()
    got = pbuf[...].astype(F32)
    own = lat_ref[:, pl.ds(pl.multiple_of(c * HD, 128), HD)].astype(F32)
    latbuf[c, chip] = jnp.concatenate(
        [jnp.where(first_core, own, got), jnp.where(first_core, got, own)], 0
    ).astype(BF16)
    gather_open(mine, lgs, lgr)
    to_partner(chip)

    mp.wait_recv()
    mbuf[z] = mpair[...] + mpair_r[...]

    def m1_send(i, carry):
        remote(mbuf.at[z], mbuf.at[z], m1s, m1r.at[z], {"sp": lax.rem(z + i, Z)}).start()
        return carry

    lax.fori_loop(1, Z, m1_send, 0)

    gather_relay(mine, lgs, lgr, to_partner)

    def m1_wait(i, s):
        k = lax.rem(z + i, Z)
        remote(mbuf.at[k], mbuf.at[k], m1s, m1r.at[k], partner).wait_recv()
        return s + mbuf[k]

    msum = lax.fori_loop(1, Z, m1_wait, mbuf[z])
    gate = msum[4:5]
    sbuf[chip] = msum[0:4]

    def m2_send(i, carry):
        k = lax.rem(chip + i, NC)
        remote(
            sbuf.at[chip], sbuf.at[chip], m2s, m2r.at[chip], {"tp_0": k // X, "tp_1": lax.rem(k, X)}
        ).start()
        return carry

    lax.fori_loop(1, NC, m2_send, 0)

    gather_close(mine, lgs, lgr, to_partner)
    wocopy.start()

    def d2d_wait(k, carry):
        remote(other.at[k], other.at[k], ld_s, ldr.at[k], partner).wait_recv()
        return carry

    lax.fori_loop(0, NC, d2d_wait, 0)

    def sq_lat(k, t):
        off = pl.ds(pl.multiple_of(k * 128, 128), 128)
        for h in range(2):
            v = latbuf[h, :, :, off].astype(F32).reshape(T, 128)
            t = t + v * v
        return t

    tot = lax.fori_loop(0, HC, sq_lat, jnp.zeros((T, 128), F32))
    r_lat = lax.rsqrt(jnp.sum(tot, axis=1, keepdims=True) / D + EPS)

    def m2_wait(i, carry):
        k = lax.rem(chip + i, NC)
        remote(sbuf.at[k], sbuf.at[k], m2s, m2r.at[k], partner).wait_recv()
        return carry

    lax.fori_loop(1, NC, m2_wait, 0)

    CH = min(4, HC)
    KB = CH * 128

    def scales(i, row):
        return jnp.concatenate([sbuf[i * CH + j][row : row + 1] for j in range(CH)], 1)

    def chunk(i):
        return i // (HC // CH), pl.multiple_of(lax.rem(i, HC // CH) * KB, 128), pl.multiple_of(i * KB, 128)

    r_first, r_last = r_lat[0:8], r_lat[T - 8 : T]

    def small(i, carry):
        h, off, at = chunk(i)
        gains = gain_ref[:, pl.ds(at, KB)].astype(F32)
        gs = gains * (1.0 + scales(i, 1))
        sh = scales(i, 0)
        gsc = gains * (1.0 + scales(i, 3))
        shc = scales(i, 2)
        vc = ctx_ref[:, pl.ds(at, KB)].astype(F32) * r_ctx * gsc + shc
        v0 = latbuf[h, 0, :, pl.ds(off, KB)].astype(F32) * r_first * gs + sh
        v1 = latbuf[h, NC - 1, :, pl.ds(off, KB)].astype(F32) * r_last * gs + sh
        rows = jnp.concatenate([vc, v0, v1], 0).astype(BF16)
        return carry + jnp.dot(rows, wcat[pl.ds(at, KB), :], preferred_element_type=F32)

    proj_s = lax.fori_loop(0, NC // CH, small, jnp.zeros((CZ + 16, 512), F32))

    lane128 = iota((128, 128), 1)
    sub128 = iota((128, 128), 0)
    sel_ctx = ((lane128 - 64 + 2 * head == sub128) & (lane128 >= 64) & (lane128 < 66)).astype(BF16)
    dt_ctx = bdot(proj_s[:CZ, 384:512], sel_ctx)
    lane_c = iota((CZ, 128), 1)
    cbuf[z] = jnp.concatenate([jnp.where(lane_c < 64, proj_s[:CZ, 0:128], dt_ctx), proj_s[:CZ, 128:256]], 1).astype(BF16)
    esend[0] = proj_s[CZ + 8 : CZ + 16, 0:384].astype(BF16)
    esend[1] = proj_s[CZ : CZ + 8, 0:384].astype(BF16)
    e_up = remote(esend.at[0], ebuf.at[0], es.at[0], er.at[0], {"sp": lax.rem(z + 1, Z)})
    e_down = remote(esend.at[1], ebuf.at[1], es.at[1], er.at[1], {"sp": lax.rem(z + Z - 1, Z)})
    e_up.start()
    e_down.start()

    def c_send(i, carry):
        remote(cbuf.at[z], cbuf.at[z], css, csr.at[z], {"sp": lax.rem(z + i, Z)}).start()
        return carry

    lax.fori_loop(1, Z, c_send, 0)

    acc[...] = jnp.zeros_like(acc)

    def main(i, carry):
        h, off, at = chunk(i)
        gs = gain_ref[:, pl.ds(at, KB)].astype(F32) * (1.0 + scales(i, 1))
        sh = scales(i, 0)
        v = latbuf[h, :, :, pl.ds(off, KB)].astype(F32).reshape(T, KB)
        rows = (v * r_lat * gs + sh).astype(BF16)
        acc[...] += jnp.dot(rows, wcat[pl.ds(at, KB), :], preferred_element_type=F32)
        return carry

    lax.fori_loop(0, NC // CH, main, 0)

    b0, b1 = dtb_ref[0], dtb_ref[1]
    d0, d1 = dlog_ref[0], dlog_ref[1]
    sel_col = (lane128 + 2 * head == sub128).astype(BF16) * (lane128 < 2).astype(BF16)
    sel_row = ((iota((8, 128), 0) + 2 * head == iota((8, 128), 1)) & (iota((8, 128), 0) < 2)).astype(BF16)
    dt_all = acc[:, 384:512].astype(BF16)
    nt = (((1,), (1,)), ((), ()))
    lane_t = iota((T, 128), 1)
    sub_8t = iota((8, T), 0)
    step_col = softplus(bdot(dt_all, sel_col) + jnp.where(lane_t == 0, b0, b1))
    step_row = softplus(bdot(sel_row, dt_all, nt) + jnp.where(sub_8t == 0, b0, b1))
    a_col = -step_col * jnp.exp(jnp.where(lane_t == 0, d0, d1))
    a_row = -step_row * jnp.exp(jnp.where(sub_8t == 0, d0, d1))
    q_i = iota((T, T), 0)
    s_i = iota((T, T), 1)
    low = (s_i <= q_i).astype(F32)
    upp = (s_i >= q_i).astype(F32)
    lf_col = hdot(low, a_col)[:, 0:1]
    lb_col = hdot(upp, a_col)[:, 1:2]
    lf_row = hdot(a_row, upp)[0:1]
    lb_row = hdot(a_row, low)[1:2]
    lf_tot = lf_col[T - 1 : T]
    lb_tot = lb_col[0:1]
    lane_1 = iota((1, 128), 1)
    lbuf[z] = jnp.where(lane_1 == 0, lf_tot, lb_tot)

    def l_send(i, carry):
        remote(lbuf.at[z], lbuf.at[z], ls_, lr_.at[z], {"sp": lax.rem(z + i, Z)}).start()
        return carry

    lax.fori_loop(1, Z, l_send, 0)

    e_up.wait_recv()
    e_down.wait_recv()

    def conv(v, before, after, taps, rows):
        n = v.shape[0]
        up = jnp.where(rows == 0, before, pltpu.roll(v, 1, 0))
        down = jnp.where(rows == n - 1, after, pltpu.roll(v, n - 1, 0))
        return silu(taps[0] * up + taps[1] * v + taps[2] * down)

    def taps_of(ref):
        rows = [ref[i : i + 1, :].astype(F32) for i in range(3)]
        if rows[0].shape[1] < 128:
            rows = [jnp.concatenate([r, jnp.zeros_like(r)], 1) for r in rows]
        return rows

    tx, tb, tc = taps_of(cx_ref), taps_of(cb_ref), taps_of(cc_ref)
    sub_t = iota((T, 128), 0)
    has_prev = (z > 0).astype(F32)
    has_next = (z < Z - 1).astype(F32)
    e_prev = ebuf[0].astype(F32)[7:8] * has_prev
    e_next = ebuf[1].astype(F32)[0:1] * has_next

    def seg(i):
        return acc[:, i * 128 : i * 128 + 128].astype(BF16).astype(F32)

    def edges(e, i):
        return e[:, i * 128 : i * 128 + 128]

    xz = seg(0)
    xs = conv(xz, edges(e_prev, 0), edges(e_next, 0), tx, sub_t)
    bs = conv(seg(1), edges(e_prev, 1), edges(e_next, 1), tb, sub_t)
    cs = conv(seg(2), edges(e_prev, 2), edges(e_next, 2), tc, sub_t)
    bs_b = bs.astype(BF16)
    cs_b = cs.astype(BF16)

    tn = (((0,), (0,)), ((), ()))

    def state_of(v, writes, wf, wb, lanes):
        doubled = v + pltpu.roll(v, 64, 1)
        return bdot(doubled * jnp.where(lanes < 64, wf, wb), writes, tn)

    st = state_of(
        xs, bs_b,
        jnp.exp(lf_tot - lf_col) * step_col[:, 0:1],
        jnp.exp(lb_tot - lb_col) * step_col[:, 1:2],
        lane_t,
    )
    snd[...] = st.reshape(2, 64, 128).astype(BF16)

    def s_send(i, carry):
        k = lax.rem(z + i, Z)
        back = (k < z).astype(jnp.int32)
        remote(snd.at[back], rst.at[z], sts, str_.at[z], {"sp": k}).start()
        return carry

    lax.fori_loop(1, Z, s_send, 0)

    pf = jnp.where(s_i <= q_i, jnp.exp(jnp.minimum(lf_col - lf_row, 0.0)), 0.0) * step_row[0:1]
    pb = jnp.where(s_i >= q_i, jnp.exp(jnp.minimum(lb_col - lb_row, 0.0)), 0.0) * step_row[1:2]
    inter = bdot(cs_b, bs_b, nt)
    y_in = bdot(inter * (pf + pb), xs)

    def c_wait(i, carry):
        k = lax.rem(z + i, Z)
        remote(cbuf.at[k], cbuf.at[k], css, csr.at[k], partner).wait_recv()
        return carry

    lax.fori_loop(1, Z, c_wait, 0)
    cin = cbuf[...].astype(F32).reshape(CT, 256)
    sub_c = iota((CT, 128), 0)
    lane_ct = iota((CT, 128), 1)
    zero_row = jnp.zeros((1, 128), F32)
    xs_c = conv(cin[:, 0:128], zero_row, zero_row, tx, sub_c)
    bs_c = conv(cin[:, 128:256], zero_row, zero_row, tb, sub_c)
    step_c = softplus(cin[:, 0:128] + jnp.where(lane_ct == 64, b0, b1))
    a_c = -step_c * jnp.exp(jnp.where(lane_ct == 64, d0, d1))
    q_c = iota((CT, CT), 0)
    s_c = iota((CT, CT), 1)
    cf_col = hdot((s_c <= q_c).astype(F32), a_c)[:, 64:65]
    cb_col = hdot((s_c >= q_c).astype(F32), a_c)[:, 65:66]
    cst[...] = state_of(
        xs_c, bs_c,
        jnp.exp(cf_col[CT - 1 : CT] - cf_col) * step_c[:, 64:65],
        jnp.exp(cb_col[0:1] - cb_col) * step_c[:, 65:66],
        lane_ct,
    )

    wocopy.wait_recv()

    def join_o(i, carry):
        rows = pl.ds(pl.multiple_of(i * RB, RB), RB)
        a, b = wo_own[rows, :], wo_part[rows, :]
        wo[rows, :] = jnp.where(first_core, jnp.concatenate([a, b], 1), jnp.concatenate([b, a], 1))
        return carry

    lax.fori_loop(0, D // RB, join_o, 0)

    def l_wait(i, carry):
        k = lax.rem(z + i, Z)
        remote(lbuf.at[k], lbuf.at[k], ls_, lr_.at[k], partner).wait_recv()
        remote(snd.at[0], rst.at[k], sts, str_.at[k], partner).wait_recv()
        return carry

    lax.fori_loop(1, Z, l_wait, 0)

    def enter(i, carry):
        sf, sb, runs = carry
        kf = lax.rem(z + Z - i, Z)
        kb = lax.rem(z + i, Z)
        okf = (i <= z).astype(F32)
        okb = (z + i < Z).astype(F32)
        w = jnp.exp(runs)
        sf = sf + (w[:, 0:1] * okf) * rst[kf].astype(F32)
        sb = sb + (w[:, 1:2] * okb) * rst[kb].astype(F32)
        runs = runs + jnp.where(lane_1 == 0, lbuf[kf] * okf, lbuf[kb] * okb)
        return sf, sb, runs

    zero_state = jnp.zeros((64, 128), F32)
    sf, sb, runs = lax.fori_loop(1, Z, enter, (zero_state, zero_state, jnp.zeros((1, 128), F32)))
    w = jnp.exp(runs)
    sf = sf + w[:, 0:1] * cst[0:64]
    sb = sb + w[:, 1:2] * cst[64:128]

    carried = bdot(cs_b, jnp.concatenate([sf, sb], 0), nt) * jnp.where(lane_t < 64, jnp.exp(lf_col), jnp.exp(lb_col))
    ys = y_in + carried + pltpu.roll(carried, 64, 1)
    zin = pltpu.roll(xz, 64, 1)
    g = jnp.where(lane_t < 64, ys * silu(zin), 0.0)
    hg = hg_ref[...].astype(F32)
    hg = jnp.concatenate([hg, jnp.zeros_like(hg)], 1)
    heads = g * lax.rsqrt(jnp.sum(g * g, axis=1, keepdims=True) / 64 + EPS) * hg
    heads = jnp.where(first_core, heads, pltpu.roll(heads, 64, 1))

    osend[...] = jnp.where(first_core, heads[TH:T], heads[0:TH]).astype(BF16)
    op = remote(osend, orecv, ops, opr, partner)
    op.start()
    keep = jnp.where(first_core, heads[0:TH], heads[TH:T])
    op.wait_recv()
    obuf[chip] = (keep + orecv[...].astype(F32)).astype(BF16)
    gather_open(obuf, ogs, ogr)
    gather_relay(obuf, ogs, ogr, lambda slot: None)
    gather_close(obuf, ogs, ogr, lambda slot: None)

    def out_dot(i, t):
        rows = jnp.concatenate([obuf[i * CH + j] for j in range(CH)], 1)
        return t + jnp.dot(rows, wo[pl.ds(pl.multiple_of(i * KB, KB), KB), :], preferred_element_type=F32)

    upd = lax.fori_loop(0, NC // CH, out_dot, jnp.zeros((TH, 128), F32)) * gate
    ubuf[...] = upd.reshape(TH // 8, 8, 128).astype(BF16)

    in_half = chip // HC == c

    def u_send(i, carry):
        j = lax.rem(lax.rem(head, NC) + i, NC)
        k = c * HC + j // 2
        e = lax.rem(j, 2)
        me = (k == chip) & (e == c)

        @pl.when(jnp.logical_not(me))
        def _():
            remote(
                ubuf.at[j // 2], rbuf.at[chip], us, ur.at[chip],
                {"tp_0": k // X, "tp_1": lax.rem(k, X), "tp_2": e},
            ).start()

        return carry

    lax.fori_loop(0, NC, u_send, 0)

    @pl.when(in_half)
    def _():
        rbuf[chip] = ubuf[lax.rem(chip, HC)]

    def u_wait(k, carry):
        @pl.when(jnp.logical_not(in_half & (k == chip)))
        def _():
            remote(ubuf.at[0], rbuf.at[k], us, ur.at[k], partner).wait_recv()

        return carry

    lax.fori_loop(0, NC, u_wait, 0)

    def finish(k, carry):
        cols = pl.ds(pl.multiple_of(k * 128, 128), 128)
        v = rbuf[k].astype(F32)
        v = jnp.where(first_core, v[0:4], v[4:8])
        out_ref[:, cols] = (lat_ref[:, cols].astype(F32) + v).astype(BF16)
        return carry

    lax.fori_loop(0, NC, finish, 0)

    lp.wait_send()
    mp.wait_send()
    wocopy.wait_send()
    e_up.wait_send()
    e_down.wait_send()
    op.wait_send()
    drain(mbuf.at[pl.ds(0, Z - 1)], m1s)
    drain(sbuf.at[pl.ds(0, NC - 1)], m2s)
    gather_drain(mine, lgs)
    drain(mine.at[pl.ds(0, NC)], ld_s)
    drain(cbuf.at[pl.ds(0, Z - 1)], css)
    drain(lbuf.at[pl.ds(0, Z - 1)], ls_)
    drain(rst.at[pl.ds(0, Z - 1)], sts)
    gather_drain(obuf, ogs)

    @pl.when(in_half)
    def _():
        drain(rbuf.at[pl.ds(0, NC - 1)], us)

    @pl.when(jnp.logical_not(in_half))
    def _():
        drain(rbuf.at[pl.ds(0, NC)], us)


def per_device(sizes, latent, context, cond, cond_ctx, wsh, wsc, wga, gain, pz, px, pb, pc, pdt, cx, cb, cc, dtb, dlog, hg, po):
    Z, Y, X = sizes
    NC = Y * X
    D = latent.shape[1]
    T = 8 * NC
    CZ = context.shape[0]
    if pdt.shape[1] < 128:
        pdt = jnp.pad(pdt, ((0, 0), (0, 128 - pdt.shape[1])))
    V = pltpu.VMEM
    S = pltpu.SemaphoreType.DMA
    vm = pl.BlockSpec(memory_space=pltpu.VMEM)
    hb = pl.BlockSpec(memory_space=pl.ANY)
    sm = pl.BlockSpec(memory_space=pltpu.SMEM)
    one = S
    return pl.pallas_call(
        functools.partial(kernel, sizes),
        out_shape=jax.ShapeDtypeStruct(latent.shape, BF16),
        in_specs=[vm, vm, vm, vm, vm, vm, vm, vm, hb, hb, hb, hb, hb, vm, vm, vm, sm, sm, vm, hb],
        out_specs=vm,
        scratch_shapes=[
            V((D, 512), BF16), V((D, 64), BF16), V((D, 64), BF16), V((D, 64), BF16), V((D, 64), BF16), V((D, 128), BF16),
            V((2, NC, 8, D // 2), BF16), V((4, D // 2), BF16), V((4, D // 2), BF16), V((5, 128), F32), V((5, 128), F32),
            V((Z, 5, 128), F32), V((NC, 4, 128), F32), V((T, 512), F32), V((8, 128), F32),
            V((Z, CZ, 256), BF16), V((2, 8, 384), BF16), V((2, 8, 384), BF16), V((Z, 1, 128), F32),
            V((2, 64, 128), BF16), V((Z, 64, 128), BF16), V((T // 2, 128), BF16), V((T // 2, 128), BF16),
            V((NC, T // 2, 128), BF16), V((T // 16, 8, 128), BF16), V((NC, 8, 128), BF16), V((128, 128), F32),
            S((6,)), one, one, one, one, one, one, one, S((Z,)), one, S((NC,)), one, S((NC,)), one, S((NC,)),
            one, S((Z,)), S((2,)), S((2,)), one, S((Z,)), one, S((Z,)), one, one, one, S((NC,)), one, S((NC,)),
        ],
        compiler_params=pltpu.CompilerParams(collective_id=0, has_side_effects=True, vmem_limit_bytes=48 << 20),
        name="mixer",
    )(
        latent, context, cond.reshape(1, -1), cond_ctx.reshape(1, -1), wsh, wsc, wga, gain.reshape(1, -1),
        pz, px, pb, pc, pdt, cx, cb, cc, dtb, dlog, hg.reshape(1, -1), po,
    )


def build(mesh, sizes):
    Z, Y, X = sizes
    torus = Mesh(mesh.devices.reshape(Z, Y, X, 2), SP_TP)
    in_specs = (
        P(SP_TP, None), P("sp", None), P("sp"), P("sp"), P("sp", TP), P("sp", TP), P("sp", TP), P(),
        P(None, TP), P(None, TP), P(None, TP), P(None, TP), P(), P(None, TP), P(None, TP), P(None, TP),
        P(TP), P(TP), P(TP), P(None, TP),
    )
    return jax.shard_map(
        functools.partial(per_device, sizes), mesh=torus, in_specs=in_specs, out_specs=P(SP_TP, None), check_vma=False
    )


def solution(mesh):
    return build(mesh, (mesh.shape["sp"], 8, 4))
```

time: 351 us -> 112 us (0.32)
  blocking collectives: 118 us -> 0 us
  Pallas kernels: 0 us -> 100 us
  waiting for transfers between devices: 86.3 us -> 0 us
  starting transfers between devices: 66.2 us -> 0 us
  other arithmetic: 21.7 us -> 0 us
  between operations: 18 us -> 0.21 us
  matrix products: 14 us -> 0 us
  local copies, waits for them, and re-layouts: 25.1 us -> 11.4 us
    pallas_call x0 -> x1, Pallas kernels: none -> 100 us  [per_device(): pl.pallas_call(functools.partial(kernel, sizes), out_shape=jax.ShapeDtype...]
    all_to_all x1 -> x0, blocking collectives: 65.7 us -> none  [copy_for_each(): return lax.all_to_all(copies, axis, split_axis=0, concat_axis=0, tiled=True)]
    all_to_all x5 -> x0, starting transfers between devices: 60.8 us -> none  [the longest x4 53.8 us: copy_for_each(): return lax.all_to_all(copies, axis, split_axis=0, concat_axis=0, tiled=True)]
    all_gather x2 -> x0, blocking collectives: 52 us -> none  [the longest x1 42.2 us: rows_first(): filled, at, outs = (lax.all_gather(both, axis, axis=0, tiled=True), 0, [])]
    all_to_all x5 -> x0, waiting for transfers between devices: 51.1 us -> none  [the longest x4 42.7 us: copy_for_each(): return lax.all_to_all(copies, axis, split_axis=0, concat_axis=0, tiled=True)]
    all_gather x2 -> x0, waiting for transfers between devices: 35.1 us -> none  [gather_in_order(): parts = lax.all_gather(parts, axes[k])]
    dot_general x22 -> x0, matrix products: 14 us -> none  [the longest x8 7.6 us: project(): jnp.dot(rows, w, preferred_element_type=jnp.float32).astype(jnp.bfloat16)]
    unnamed x62 -> x39, local copies, waits for them, and re-layouts: 2.53 us -> 10.7 us
  transfers between devices with their start and end apart: 9 -> 0, of which waited for: 7 -> 0; matrix products, arithmetic and copies ran while one was open for 6% -> 0% of each run, Pallas kernels for 0% -> 0%
where the time goes in v1:
time: 112 us
  Pallas kernels  100 us (89%)
  local copies, waits for them, and re-layouts  11.4 us (10%)
    pallas_call x1, Pallas kernels, per_device(): pl.pallas_call(functools.partial(kernel, sizes), out_shape=jax.ShapeDtype...  100 us
    unnamed x39, local copies, waits for them, and re-layouts  10.7 us

profile of v1, /device:TPU:1, one launch (start us, length us, event | category | flops | bytes accessed | tf_op | source)
XLA Modules:
  0.0 111.8 jit_solution(3768901823816791001)
XLA Ops:
  0.0 0.7 copy-done.14
  0.7 0.6 copy-done.15
  1.3 0.7 reshape.14.gain_ref
  2.0 0.0 copy-start.12
  2.0 0.9 copy.21.wsh_ref
  2.9 0.0 copy-start.13
  2.9 0.1 copy.22.wsc_ref
  3.1 0.6 copy-done.13
  3.7 0.1 copy.23.wga_ref
  3.8 0.0 copy-start.11
  3.8 1.6 %copy.24.pz_ref = bf16[4096,64]{1,0:T(8,128)(2,1)S(1)} copy(bf16[4096,64]{0,1:T(8,128)(2,1)} %param.28) | data formatting | bytes 1048576 | tf_op args[8]
  5.4 0.5 copy.25.px_ref
  5.9 0.0 copy-start
  5.9 0.0 copy-start.3
  5.9 0.0 copy-start.4
  5.9 0.0 copy-start.5
  5.9 0.0 copy-start.6
  6.0 0.0 copy-start.7
  6.0 0.0 copy-start.8
  6.0 0.0 copy-start.9
  6.0 0.0 copy-start.10
  6.0 2.4 %copy.26.po_ref = bf16[4096,64]{1,0:T(8,128)(2,1)} copy(bf16[4096,64]{0,1:T(8,128)(2,1)} %param.39) | data formatting | bytes 1048576 | tf_op args[19]
  8.5 0.0 copy-done.5
  8.5 0.0 copy-done.6
  8.5 0.0 copy-done.7
  8.5 0.0 copy-done.8
  8.5 0.0 copy-done.9
  8.5 0.0 copy-start.1
  8.5 1.2 %copy-done.1 = bf16[4096,128]{1,0:T(8,128)(2,1)S(1)} copy-done((bf16[4096,128]{1,0:T(8,128)(2,1)S(1)}, bf16[4096,128]{1,0:T(8,128)(2,1)}, u32[]{:S(2)}) %copy-start.1) | copy-done | bytes 1048600
  9.8 1.2 %copy-done.2 = bf16[4096,128]{1,0:T(8,128)(2,1)S(1)} copy-done((bf16[4096,128]{1,0:T(8,128)(2,1)S(1)}, bf16[4096,128]{1,0:T(8,128)(2,1)}, u32[]{:S(2)}) %copy-start.2) | copy-done | bytes 1048600
  11.0 100.2 %mixer.1 = bf16[4,4096]{1,0:T(4,128)(2,1)S(1)} custom-call(bf16[4,4096]{1,0:T(4,128)(2,1)S(1)} %copy-done.4, bf16[16,4096]{1,0:T(8,128)(2,1)S(1)} %copy-done.3, bf16[1,256]{1,0:T(2,128)(2,1)S(1)} %reshape.12.cond_ref, bf16[1,256]{1,0:T(2,128)(2,1)S(1)} %reshape.13.condc_ref, bf16[256,64]{1,0:T(8,128)(2,1)S(1)} %copy.21.wsh_ref, ...), custom_call_target="tpu_custom_call" | custom-call | tf_op jit(solution)/shard_map/mixer/pallas_call | solution.py:585
  111.2 0.6 copy.28
  (11 shorter events, 0.0 us)
Async XLA Ops:
  0.0 0.7 copy-start.14
  0.7 0.7 copy-start.15
  2.0 0.9 copy-start.12
  2.9 0.8 copy-start.13
  3.8 1.6 %copy-start.11 = (bf16[4096,64]{0,1:T(8,128)(2,1)S(1)}, bf16[4096,64]{0,1:T(8,128)(2,1)}, u32[]{:S(2)}) copy-start(bf16[4096,64]{0,1:T(8,128)(2,1)} %param.29) | copy-start | bytes 1572868
  5.9 2.6 %copy-start = (bf16[4096,128]{1,0:T(8,128)(2,1)S(1)}, bf16[4096,128]{1,0:T(8,128)(2,1)}, u32[]{:S(2)}) copy-start(bf16[4096,128]{1,0:T(8,128)(2,1)} %pb_ref.1) | copy-start | bytes 3145732
  5.9 2.5 %copy-start.3 = (bf16[16,4096]{1,0:T(8,128)(2,1)S(1)}, bf16[16,4096]{1,0:T(8,128)(2,1)}, u32[]{:S(2)}) copy-start(bf16[16,4096]{1,0:T(8,128)(2,1)} %ctx_ref.1) | copy-start | bytes 393220
  5.9 2.5 %copy-start.4 = (bf16[4,4096]{1,0:T(4,128)(2,1)S(1)}, bf16[4,4096]{1,0:T(4,128)(2,1)}, u32[]{:S(2)}) copy-start(bf16[4,4096]{1,0:T(4,128)(2,1)} %lat_ref.1) | copy-start | bytes 98308
  5.9 2.5 %copy-start.5 = (bf16[3,64]{1,0:T(4,128)(2,1)S(1)}, bf16[3,64]{1,0:T(4,128)(2,1)}, u32[]{:S(2)}) copy-start(bf16[3,64]{1,0:T(4,128)(2,1)} %cx_ref.1) | copy-start | bytes 1156
  5.9 2.5 %copy-start.6 = (bf16[3,128]{1,0:T(4,128)(2,1)S(1)}, bf16[3,128]{1,0:T(4,128)(2,1)}, u32[]{:S(2)}) copy-start(bf16[3,128]{1,0:T(4,128)(2,1)} %cb_ref.1) | copy-start | bytes 2308
  6.0 2.5 %copy-start.7 = (bf16[3,128]{1,0:T(4,128)(2,1)S(1)}, bf16[3,128]{1,0:T(4,128)(2,1)}, u32[]{:S(2)}) copy-start(bf16[3,128]{1,0:T(4,128)(2,1)} %cc_ref.1) | copy-start | bytes 2308
  6.0 2.5 %copy-start.8 = (f32[2]{0:T(128)S(1)}, f32[2]{0:T(128)}, u32[]{:S(2)}) copy-start(f32[2]{0:T(128)} %dtb_ref.1) | copy-start | bytes 28
  6.0 2.5 %copy-start.9 = (f32[2]{0:T(128)S(1)}, f32[2]{0:T(128)}, u32[]{:S(2)}) copy-start(f32[2]{0:T(128)} %dlog_ref.1) | copy-start | bytes 28
  6.0 2.5 %copy-start.10 = (bf16[64]{0:T(256)(128)(2,1)S(1)}, bf16[64]{0:T(256)(128)(2,1)}, u32[]{:S(2)}) copy-start(bf16[64]{0:T(256)(128)(2,1)} %param.38) | copy-start | bytes 388
  8.5 1.2 %copy-start.1 = (bf16[4096,128]{1,0:T(8,128)(2,1)S(1)}, bf16[4096,128]{1,0:T(8,128)(2,1)}, u32[]{:S(2)}) copy-start(bf16[4096,128]{1,0:T(8,128)(2,1)} %pc_ref.1) | copy-start | bytes 3145732
  9.7 1.2 %copy-start.2 = (bf16[4096,128]{1,0:T(8,128)(2,1)S(1)}, bf16[4096,128]{1,0:T(8,128)(2,1)}, u32[]{:S(2)}) copy-start(bf16[4096,128]{1,0:T(8,128)(2,1)} %pdt_ref.1) | copy-start | bytes 3145732

commit v2 on v1

v2 whole, which is shorter than its diff:
```python
import functools

import jax
import jax.numpy as jnp
from jax import lax
from jax.experimental import pallas as pl
from jax.experimental.pallas import tpu as pltpu
from jax.sharding import Mesh
from jax.sharding import PartitionSpec as P

TP = ("tp_0", "tp_1", "tp_2")
SP_TP = ("sp", "tp_0", "tp_1", "tp_2")
EPS = 1e-06
MESH_ID = pl.DeviceIdType.MESH
F32 = jnp.float32
BF16 = jnp.bfloat16
HI = lax.Precision.HIGHEST


def iota(shape, dim):
    return lax.broadcasted_iota(jnp.int32, shape, dim)


def silu(v):
    return v * (1.0 / (1.0 + jnp.exp(-v)))


def softplus(v):
    return jnp.maximum(v, 0.0) + jnp.log1p(jnp.exp(-jnp.abs(v)))


def bdot(a, b, dims=(((1,), (0,)), ((), ()))):
    return lax.dot_general(a.astype(BF16), b.astype(BF16), dims, preferred_element_type=F32)


def hdot(a, b):
    return jnp.dot(a, b, precision=HI, preferred_element_type=F32)


def kernel(
    sizes,
    lat_h, ctx_h, cond_h, condc_h, wsh_h, wsc_h, wga_h, gain_h,
    pz_ref, px_ref, pb_ref, pc_ref, pdt_ref, cx_h, cb_h, cc_h, dtb_h, dlog_h, hg_h, po_ref,
    out_ref,
    lat_ref, ctx_ref, cond_ref, condc_ref, wsh_ref, wsc_ref, wga_ref, gain_ref,
    cx_ref, cb_ref, cc_ref, dtb_ref, dlog_ref, hg_ref,
    wcat, wxz, wot, wo, latbuf, pbuf, psend, mpair, mpair_r, mbuf, sbuf, acc, acco,
    cbuf, ebuf, esend, lbuf, snd, rst, osend, orecv, obuf, ubuf, rbuf, cst, ssq,
    wsem, wosem, worsem, pss, prs, mps, mpr, m1s, m1r, m2s, m2r, lgs, lgy, lgx, ld_s, ldr,
    css, csr, es, er, ls_, lr_, sts, str_, ops, opr, ogs, ogy, ogx, us, ur,
):
    Z, Y, X = sizes
    NC = Y * X
    HC = NC // 2
    D = lat_ref.shape[1]
    HD = D // 2
    HQ = D // 4
    T = NC * 8
    TH = T // 2
    CZ = ctx_ref.shape[0]
    CT = CZ * Z
    z = lax.axis_index("sp")
    y = lax.axis_index("tp_0")
    x = lax.axis_index("tp_1")
    c = lax.axis_index("tp_2")
    chip = y * X + x
    head = chip * 2 + c
    first_core = c == 0

    def remote(src, dst, ssem, rsem, dev):
        return pltpu.make_async_remote_copy(
            src_ref=src, dst_ref=dst, send_sem=ssem, recv_sem=rsem, device_id=dev, device_id_type=MESH_ID
        )

    def drain(buf, n, sem):
        if n:
            ref = buf.at[pl.ds(0, n)]
            pltpu.make_async_copy(ref, ref, sem).wait()

    partner = {"tp_2": 1 - c}

    wot_own = wot.at[pl.ds(pl.multiple_of(c * 64, 64), 64)]
    moves = [
        (lat_h, lat_ref), (wsh_h, wsh_ref), (wsc_h, wsc_ref), (wga_h, wga_ref), (cond_h, cond_ref), (condc_h, condc_ref),
        (ctx_h, ctx_ref), (gain_h, gain_ref), (cx_h, cx_ref), (cb_h, cb_ref), (cc_h, cc_ref),
        (dtb_h, dtb_ref), (dlog_h, dlog_ref), (hg_h, hg_ref),
        (po_ref, wot_own), (px_ref, wxz.at[0:64]), (pz_ref, wxz.at[64:128]),
        (pb_ref, wcat.at[:, 128:256]), (pc_ref, wcat.at[:, 256:384]), (pdt_ref, wcat.at[:, 384:512]),
    ]
    loads = [pltpu.make_async_copy(a, b, wsem.at[i]) for i, (a, b) in enumerate(moves)]
    for load in loads:
        load.start()

    bar = pltpu.get_barrier_semaphore()

    def hello(dev):
        pl.semaphore_signal(bar, inc=1, device_id=dev, device_id_type=MESH_ID)

    def greet_z(i, carry):
        hello({"sp": lax.rem(z + i, Z)})
        return carry

    def greet_row(i, carry):
        yy = lax.rem(y + i, Y)
        for d in range(X):
            xx = lax.rem(x + d, X)
            hello({"tp_0": yy, "tp_1": xx})
            hello({"tp_0": yy, "tp_1": xx, "tp_2": 1 - c})
        return carry

    hello(partner)
    for d in range(1, X):
        xx = lax.rem(x + d, X)
        hello({"tp_1": xx})
        hello({"tp_1": xx, "tp_2": 1 - c})
    lax.fori_loop(1, Y, greet_row, 0)
    lax.fori_loop(1, Z, greet_z, 0)

    nt = (((1,), (1,)), ((), ()))
    tn = (((0,), (0,)), ((), ()))

    loads[0].wait()
    lat = lat_ref[...].astype(F32)
    psend[...] = jnp.where(first_core, lat[:, HD:], lat[:, :HD]).astype(BF16)

    for load in loads[1:6]:
        load.wait()

    def line(ref):
        v = ref[...].astype(F32)
        return jnp.concatenate([v[k : k + 1] for k in range(ref.shape[0])], 1)

    row8 = iota((8, cond_ref.shape[0] * cond_ref.shape[1]), 0)
    both = jnp.where(row8 == 0, line(cond_ref), jnp.where(row8 == 1, line(condc_ref), 0.0))
    act = silu(both).astype(BF16)

    def wide(part):
        zero = jnp.zeros_like(part)
        return jnp.where(first_core, jnp.concatenate([part, zero], 1), jnp.concatenate([zero, part], 1))

    psh = wide(bdot(act, wsh_ref[...], nt))
    psc = wide(bdot(act, wsc_ref[...], nt))
    pga = wide(bdot(act, wga_ref[...], nt))
    mpair[...] = jnp.concatenate([psh[0:1], psc[0:1], psh[1:2], psc[1:2], pga[0:1]], 0)

    pl.semaphore_wait(bar, Z - 1 + NC * 2 - 1)

    lp = remote(psend, pbuf, pss, prs, partner)
    lp.start()
    mp = remote(mpair, mpair_r, mps, mpr, partner)
    mp.start()
    wocopy = remote(wot_own, wot_own, wosem, worsem, partner)

    def far_first(i):
        return Z // 2 + (1 - 2 * lax.rem(i, 2)) * ((i + 1) // 2)

    def near(n):
        return [d for k in range(1, (n + 1) // 2) for d in (k, n - k)] + ([n // 2] if n % 2 == 0 else [])

    def gather(buf, ssem, ysem, xsem, middle, row_done):
        def x_send(row):
            slot = buf.at[row * X + x]
            for d in near(X):
                remote(slot, slot, ssem, xsem.at[row], {"tp_1": lax.rem(x + d, X)}).start()

        def x_take(row):
            drain(buf, X - 1, xsem.at[row])
            row_done(row)

        own = buf.at[chip]
        x_send(y)
        for d in near(Y):
            remote(own, own, ssem, ysem.at[y], {"tp_0": lax.rem(y + d, Y)}).start()
        rows = [y]
        for n, d in enumerate(near(Y)):
            row = lax.rem(y + Y - d, Y)
            slot = buf.at[row * X + x]
            remote(slot, slot, ssem, ysem.at[row], partner).wait_recv()
            x_send(row)
            rows.append(row)
            if n in (3, 5):
                x_take(rows.pop(0))
        middle()
        for row in rows:
            x_take(row)

    mine = latbuf.at[c]
    other = latbuf.at[1 - c]

    def squares(h, row):
        for j in range(X):
            v = latbuf[h, row * X + j].astype(F32)
            v = v * v
            t = v[0] + v[1]
            ssq[h, row * X + j] = sum(t[:, k * 128 : k * 128 + 128] for k in range(HQ // 128))

    late = []

    def row_of(ref, row):
        return ref.at[pl.ds(row * X, X)]

    def from_partner():
        row = late.pop(0)
        remote(row_of(other, row), row_of(other, row), ld_s, ldr.at[row], partner).wait_recv()
        squares(1 - c, row)

    def to_partner(row):
        remote(row_of(mine, row), row_of(mine, row), ld_s, ldr.at[row], partner).start()
        squares(c, row)
        late.append(row)
        if len(late) > 2:
            from_partner()

    lp.wait_recv()
    got = pbuf[...].astype(F32)
    own = jnp.where(first_core, lat[:, :HD], lat[:, HD:])
    block = jnp.concatenate([jnp.where(first_core, own, got), jnp.where(first_core, got, own)], 0).astype(BF16)
    latbuf[c, chip, 0] = block[:, :HQ]
    latbuf[c, chip, 1] = block[:, HQ:]

    mp.wait_recv()
    mbuf[z] = mpair[...] + mpair_r[...]

    def m1_send(i, carry):
        remote(mbuf.at[z], mbuf.at[z], m1s, m1r, {"sp": lax.rem(z + far_first(i), Z)}).start()
        return carry

    lax.fori_loop(0, Z - 1, m1_send, 0)

    def m2_send(yy, xx):
        remote(sbuf.at[chip], sbuf.at[chip], m2s, m2r, {"tp_0": yy, "tp_1": xx}).start()

    def m2_row(i, carry):
        yy = lax.rem(y + i, Y)
        for d in range(X):
            m2_send(yy, lax.rem(x + d, X))
        return carry

    def modulation():
        drain(mbuf, Z - 1, m1r)
        msum = sum(mbuf[k] for k in range(Z))
        mp.wait_send()
        mpair[...] = msum
        sbuf[chip] = msum[0:4]
        lax.fori_loop(1, Y, m2_row, 0)
        for d in range(1, X):
            m2_send(y, lax.rem(x + d, X))

    scale_of = {}

    def middle():
        modulation()
        for load in loads[6:]:
            load.wait()

        def join_w(i, carry):
            span = pl.ds(pl.multiple_of(i * 128, 128), 128)
            wcat[span, 0:128] = wxz[:, span].T
            return carry

        lax.fori_loop(0, D // 128, join_w, 0)
        def sq_ctx(k, tot):
            v = ctx_ref[:, pl.ds(pl.multiple_of(k * 128, 128), 128)].astype(F32)
            return tot + v * v

        tot = lax.fori_loop(0, NC, sq_ctx, jnp.zeros((CZ, 128), F32))
        scale_of[0] = lax.rsqrt(jnp.sum(tot, axis=1, keepdims=True) / D + EPS)

        wocopy.start()

    gather(mine, lgs, lgy, lgx, middle, to_partner)
    r_ctx = scale_of[0]

    while late:
        from_partner()
    tot = (ssq[0] + ssq[1]).reshape(T, 128)
    r_lat = lax.rsqrt(jnp.sum(tot, axis=1, keepdims=True) / D + EPS)

    drain(sbuf, NC - 1, m2r)

    CH = min(4, NC // 4)
    KB = CH * 128
    NQ = HQ // KB

    def scales(i, row):
        return jnp.concatenate([sbuf[i * CH + j][row : row + 1] for j in range(CH)], 1)

    gains_all = gain_ref[...].astype(F32)

    def gains_of(i):
        return jnp.concatenate([gains_all[i * CH + j : i * CH + j + 1] for j in range(CH)], 1)

    def chunk(i):
        return i // (2 * NQ), i // NQ % 2, i % NQ * KB, i * KB

    def small(i, carry):
        h, q, off, at = chunk(i)
        gains = gains_of(i)
        gs = gains * (1.0 + scales(i, 1))
        sh = scales(i, 0)
        gsc = gains * (1.0 + scales(i, 3))
        shc = scales(i, 2)
        vc = ctx_ref[:, pl.ds(at, KB)].astype(F32) * r_ctx * gsc + shc
        v0 = latbuf[h, 0, q, :, pl.ds(off, KB)].astype(F32) * r_lat[0:8] * gs + sh
        v1 = latbuf[h, NC - 1, q, :, pl.ds(off, KB)].astype(F32) * r_lat[T - 8 : T] * gs + sh
        rows = jnp.concatenate([vc, v0, v1], 0).astype(BF16)
        return carry + jnp.dot(rows, wcat[pl.ds(at, KB), :], preferred_element_type=F32)

    proj_s = jnp.zeros((CZ + 16, 512), F32)
    for i in range(NC // CH):
        proj_s = small(i, proj_s)

    lane128 = iota((128, 128), 1)
    sub128 = iota((128, 128), 0)
    sel_ctx = ((lane128 - 64 + 2 * head == sub128) & (lane128 >= 64) & (lane128 < 66)).astype(BF16)
    dt_ctx = bdot(proj_s[:CZ, 384:512], sel_ctx)
    lane_c = iota((CZ, 128), 1)
    cbuf[z] = jnp.concatenate([jnp.where(lane_c < 64, proj_s[:CZ, 0:128], dt_ctx), proj_s[:CZ, 128:256]], 1).astype(BF16)
    esend[0] = proj_s[CZ + 8 : CZ + 16, 0:384].astype(BF16)
    esend[1] = proj_s[CZ : CZ + 8, 0:384].astype(BF16)
    e_up = remote(esend.at[0], ebuf.at[0], es.at[0], er.at[0], {"sp": lax.rem(z + 1, Z)})
    e_down = remote(esend.at[1], ebuf.at[1], es.at[1], er.at[1], {"sp": lax.rem(z + Z - 1, Z)})
    e_up.start()
    e_down.start()

    c_first = remote(cbuf.at[z], cbuf.at[z], css.at[0], csr, {"sp": jnp.int32(0)})
    c_last = remote(cbuf.at[z], cbuf.at[z], css.at[1], csr, {"sp": jnp.int32(Z - 1)})

    @pl.when(z > 0)
    def _():
        c_first.start()

    @pl.when(z < Z - 1)
    def _():
        c_last.start()

    def main(i, total):
        h, q, off, at = chunk(i)
        gs = gains_of(i) * (1.0 + scales(i, 1))
        sh = scales(i, 0)
        v = latbuf[h, :, q, :, pl.ds(off, KB)].astype(F32).reshape(T, KB)
        rows = (v * r_lat * gs + sh).astype(BF16)
        return total + jnp.dot(rows, wcat[pl.ds(at, KB), :], preferred_element_type=F32)

    total = jnp.zeros((T, 512), F32)
    for i in range(NC // CH):
        total = main(i, total)
    acc[...] = total

    b0, b1 = dtb_ref[:, 0:1], dtb_ref[:, 1:2]
    d0, d1 = dlog_ref[:, 0:1], dlog_ref[:, 1:2]
    sel_col = (lane128 + 2 * head == sub128).astype(BF16) * (lane128 < 2).astype(BF16)
    sel_row = ((iota((8, 128), 0) + 2 * head == iota((8, 128), 1)) & (iota((8, 128), 0) < 2)).astype(BF16)
    dt_all = acc[:, 384:512].astype(BF16)
    lane_t = iota((T, 128), 1)
    sub_8t = iota((8, T), 0)
    step_col = softplus(bdot(dt_all, sel_col) + jnp.where(lane_t == 0, b0, b1))
    step_row = softplus(bdot(sel_row, dt_all, nt) + jnp.where(sub_8t == 0, b0, b1))
    a_col = -step_col * jnp.exp(jnp.where(lane_t == 0, d0, d1))
    a_row = -step_row * jnp.exp(jnp.where(sub_8t == 0, d0, d1))
    q_i = iota((T, T), 0)
    s_i = iota((T, T), 1)
    low = (s_i <= q_i).astype(BF16)
    upp = (s_i >= q_i).astype(BF16)

    def split(v):
        hi = v.astype(BF16)
        rest = v - hi.astype(F32)
        mid = rest.astype(BF16)
        return hi, mid, (rest - mid.astype(F32)).astype(BF16)

    def sums_down(mask, v):
        return sum(jnp.dot(mask, p, preferred_element_type=F32) for p in split(v))

    cum_col = sums_down(low, a_col)
    cum_row = sum(jnp.dot(p, upp, preferred_element_type=F32) for p in split(a_row))
    lf_col = cum_col[:, 0:1]
    lf_tot = cum_col[T - 1 : T, 0:1]
    lb_tot = cum_col[T - 1 : T, 1:2]
    lb_col = lb_tot - cum_col[:, 1:2] + a_col[:, 1:2]
    lf_row = cum_row[0:1]
    lb_row = lb_tot - cum_row[1:2] + a_row[1:2]
    lane_1 = iota((1, 128), 1)
    lbuf[z] = jnp.where(lane_1 == 0, lf_tot, lb_tot)

    def l_send(i, carry):
        remote(lbuf.at[z], lbuf.at[z], ls_, lr_, {"sp": lax.rem(z + far_first(i), Z)}).start()
        return carry

    lax.fori_loop(0, Z - 1, l_send, 0)

    e_up.wait_recv()
    e_down.wait_recv()

    def conv(v, before, after, taps, rows):
        n = v.shape[0]
        up = jnp.where(rows == 0, before, pltpu.roll(v, 1, 0))
        down = jnp.where(rows == n - 1, after, pltpu.roll(v, n - 1, 0))
        return silu(taps[0] * up + taps[1] * v + taps[2] * down)

    def taps_of(ref):
        rows = [ref[i : i + 1, :].astype(F32) for i in range(3)]
        if rows[0].shape[1] < 128:
            rows = [jnp.concatenate([r, jnp.zeros_like(r)], 1) for r in rows]
        return rows

    tx, tb, tc = taps_of(cx_ref), taps_of(cb_ref), taps_of(cc_ref)
    sub_t = iota((T, 128), 0)
    has_prev = (z > 0).astype(F32)
    has_next = (z < Z - 1).astype(F32)
    e_prev = ebuf[0].astype(F32)[7:8] * has_prev
    e_next = ebuf[1].astype(F32)[0:1] * has_next

    def seg(i):
        return acc[:, i * 128 : i * 128 + 128].astype(BF16).astype(F32)

    def edges(e, i):
        return e[:, i * 128 : i * 128 + 128]

    xz = seg(0)
    xs = conv(xz, edges(e_prev, 0), edges(e_next, 0), tx, sub_t)
    bs = conv(seg(1), edges(e_prev, 1), edges(e_next, 1), tb, sub_t)
    cs = conv(seg(2), edges(e_prev, 2), edges(e_next, 2), tc, sub_t)
    bs_b = bs.astype(BF16)
    cs_b = cs.astype(BF16)


    def state_of(v, writes, wf, wb, lanes):
        doubled = v + pltpu.roll(v, 64, 1)
        return bdot(doubled * jnp.where(lanes < 64, wf, wb), writes, tn)

    st = state_of(
        xs, bs_b,
        jnp.exp(lf_tot - lf_col) * step_col[:, 0:1],
        jnp.exp(lb_tot - lb_col) * step_col[:, 1:2],
        lane_t,
    )
    snd[...] = st.reshape(2, 64, 128).astype(BF16)
    cst[...] = jnp.zeros_like(cst)

    @pl.when((z == 0) | (z == Z - 1))
    def _():
        drain(cbuf, Z - 1, csr)
        cin = cbuf[...].astype(F32).reshape(CT, 256)
        sub_c = iota((CT, 128), 0)
        lane_ct = iota((CT, 128), 1)
        zero_row = jnp.zeros((1, 128), F32)
        xs_c = conv(cin[:, 0:128], zero_row, zero_row, tx, sub_c)
        bs_c = conv(cin[:, 128:256], zero_row, zero_row, tb, sub_c)
        step_c = softplus(cin[:, 0:128] + jnp.where(lane_ct == 64, b0, b1))
        a_c = -step_c * jnp.exp(jnp.where(lane_ct == 64, d0, d1))
        q_c = iota((CT, CT), 0)
        s_c = iota((CT, CT), 1)
        cf_col = sums_down((s_c <= q_c).astype(BF16), a_c)[:, 64:65]
        cb_col = sums_down((s_c >= q_c).astype(BF16), a_c)[:, 65:66]
        states = state_of(
            xs_c, bs_c,
            jnp.exp(cf_col[CT - 1 : CT] - cf_col) * step_c[:, 64:65],
            jnp.exp(cb_col[0:1] - cb_col) * step_c[:, 65:66],
            lane_ct,
        )
        cst[...] = states
        snd[...] = (st + states * jnp.where(sub128 < 64, jnp.exp(lf_tot), jnp.exp(lb_tot))).reshape(2, 64, 128).astype(BF16)

    def s_send(i, carry):
        k = lax.rem(z + far_first(i), Z)
        back = (k < z).astype(jnp.int32)
        remote(snd.at[back], rst.at[z], sts, str_, {"sp": k}).start()
        return carry

    lax.fori_loop(0, Z - 1, s_send, 0)

    pf = jnp.where(s_i <= q_i, jnp.exp(jnp.minimum(lf_col - lf_row, 0.0)), 0.0) * step_row[0:1]
    pb = jnp.where(s_i >= q_i, jnp.exp(jnp.minimum(lb_col - lb_row, 0.0)), 0.0) * step_row[1:2]
    inter = bdot(cs_b, bs_b, nt)
    y_in = bdot(inter * (pf + pb), xs)

    wocopy.wait_recv()

    def join_o(i, carry):
        span = pl.ds(pl.multiple_of(i * 128, 128), 128)
        wo[span, :] = wot[:, span].T
        return carry

    lax.fori_loop(0, D // 128, join_o, 0)

    drain(lbuf, Z - 1, lr_)
    drain(rst, Z - 1, str_)

    sf = cst[0:64] * (z == 0).astype(F32)
    sb = cst[64:128] * (z == Z - 1).astype(F32)
    runs = jnp.zeros((1, 128), F32)
    for i in range(1, Z):
        kf = lax.rem(z + Z - i, Z)
        kb = lax.rem(z + i, Z)
        okf = (i <= z).astype(F32)
        okb = (z + i < Z).astype(F32)
        w = jnp.exp(runs)
        sf = sf + (w[:, 0:1] * okf) * rst[kf].astype(F32)
        sb = sb + (w[:, 1:2] * okb) * rst[kb].astype(F32)
        runs = runs + jnp.where(lane_1 == 0, lbuf[kf] * okf, lbuf[kb] * okb)

    carried = bdot(cs_b, jnp.concatenate([sf, sb], 0), nt) * jnp.where(lane_t < 64, jnp.exp(lf_col), jnp.exp(lb_col))
    ys = y_in + carried + pltpu.roll(carried, 64, 1)
    zin = pltpu.roll(xz, 64, 1)
    g = jnp.where(lane_t < 64, ys * silu(zin), 0.0)
    hg = hg_ref[...].astype(F32)
    hg = jnp.concatenate([hg, jnp.zeros_like(hg)], 1)
    heads = g * lax.rsqrt(jnp.sum(g * g, axis=1, keepdims=True) / 64 + EPS) * hg
    heads = jnp.where(first_core, heads, pltpu.roll(heads, 64, 1))

    osend[...] = jnp.where(first_core, heads[TH:T], heads[0:TH]).astype(BF16)
    op = remote(osend, orecv, ops, opr, partner)
    op.start()
    keep = jnp.where(first_core, heads[0:TH], heads[TH:T])
    op.wait_recv()
    joined = (keep + orecv[...].astype(F32)).astype(BF16)
    obuf[chip] = joined
    acco[...] = jnp.zeros_like(acco)

    def row_dot(row):
        rows = jnp.concatenate([obuf[row * X + j] for j in range(X)], 1)
        span = pl.ds(pl.multiple_of(row * (X * 128), 128), X * 128)
        acco[...] += jnp.dot(rows, wo[span, :], preferred_element_type=F32)

    gather(obuf, ogs, ogy, ogx, lambda: None, row_dot)
    upd = acco[...] * mpair[4:5]
    ubuf[...] = upd.reshape(TH // 8, 8, 128).astype(BF16)

    in_half = chip // HC == c

    def u_row(i, carry):
        r = lax.rem(lax.rem(y, Y // 2) + i, Y // 2)
        yy = c * (Y // 2) + r
        for d in range(X):
            xx = lax.rem(x + d, X)
            for e in range(2):
                copy = remote(
                    ubuf.at[r * X + xx], rbuf.at[chip], us, ur,
                    {"tp_0": yy, "tp_1": xx, "tp_2": c if e == 0 else 1 - c},
                )
                if d == 0 and e == 0:

                    @pl.when(yy != y)
                    def _():
                        copy.start()
                else:
                    copy.start()
        return carry

    lax.fori_loop(0, Y // 2, u_row, 0)

    @pl.when(in_half)
    def _():
        rbuf[chip] = ubuf[lax.rem(chip, HC)]

    @pl.when(in_half)
    def _():
        drain(rbuf, NC - 1, ur)

    @pl.when(jnp.logical_not(in_half))
    def _():
        drain(rbuf, NC, ur)

    def finish(k, carry):
        cols = pl.ds(pl.multiple_of(k * 128, 128), 128)
        v = rbuf[k].astype(F32)
        v = jnp.where(first_core, v[0:4], v[4:8])
        out_ref[:, cols] = (lat_ref[:, cols].astype(F32) + v).astype(BF16)
        return carry

    lax.fori_loop(0, NC, finish, 0)

    lp.wait_send()
    wocopy.wait_send()
    e_up.wait_send()
    e_down.wait_send()
    op.wait_send()
    drain(mbuf, Z - 1, m1s)
    drain(sbuf, NC - 1, m2s)
    drain(mine, NC - 1, lgs)
    drain(mine, NC, ld_s)

    @pl.when(z > 0)
    def _():
        c_first.wait_send()

    @pl.when(z < Z - 1)
    def _():
        c_last.wait_send()

    drain(lbuf, Z - 1, ls_)
    drain(rst, Z - 1, sts)
    drain(obuf, NC - 1, ogs)

    @pl.when(in_half)
    def _():
        drain(rbuf, NC - 1, us)

    @pl.when(jnp.logical_not(in_half))
    def _():
        drain(rbuf, NC, us)


def per_device(sizes, latent, context, cond, cond_ctx, wsh, wsc, wga, gain, pz, px, pb, pc, pdt, cx, cb, cc, dtb, dlog, hg, po):
    Z, Y, X = sizes
    NC = Y * X
    D = latent.shape[1]
    T = 8 * NC
    CZ = context.shape[0]
    if pdt.shape[1] < 128:
        pdt = jnp.pad(pdt, ((0, 0), (0, 128 - pdt.shape[1])))
    V = pltpu.VMEM

    def lines(v):
        return (v.size // 128, 128)

    S = pltpu.SemaphoreType.DMA
    vm = pl.BlockSpec(memory_space=pltpu.VMEM)
    hb = pl.BlockSpec(memory_space=pl.ANY)
    one = S
    return pl.pallas_call(
        functools.partial(kernel, sizes),
        out_shape=jax.ShapeDtypeStruct(latent.shape, BF16),
        in_specs=[hb] * 20,
        out_specs=vm,
        scratch_shapes=[
            V((4, D), BF16), V((CZ, D), BF16), V(lines(cond), BF16), V(lines(cond), BF16),
            V((64, D // Z), BF16), V((64, D // Z), BF16), V((64, D // Z), BF16), V(lines(gain), BF16),
            V((3, 64), BF16), V((3, 128), BF16), V((3, 128), BF16), V((1, 2), F32), V((1, 2), F32), V((1, 64), BF16),
            V((D, 512), BF16), V((128, D), BF16), V((128, D), BF16), V((D, 128), BF16),
            V((2, NC, 2, 8, D // 4), BF16), V((4, D // 2), BF16), V((4, D // 2), BF16), V((5, 128), F32), V((5, 128), F32),
            V((Z, 5, 128), F32), V((NC, 4, 128), F32), V((T, 512), F32), V((T // 2, 128), F32),
            V((Z, CZ, 256), BF16), V((2, 8, 384), BF16), V((2, 8, 384), BF16), V((Z, 1, 128), F32),
            V((2, 64, 128), BF16), V((Z, 64, 128), BF16), V((T // 2, 128), BF16), V((T // 2, 128), BF16),
            V((NC, T // 2, 128), BF16), V((T // 16, 8, 128), BF16), V((NC, 8, 128), BF16), V((128, 128), F32), V((2, NC, 8, 128), F32),
            S((20,)), one, one, one, one, one, one, one, one, one, one, one, S((Y,)), S((Y,)), one, S((Y,)),
            S((2,)), one, S((2,)), S((2,)), one, one, one, one, one, one, one, S((Y,)), S((Y,)), one, one,
        ],
        compiler_params=pltpu.CompilerParams(collective_id=0, has_side_effects=True),
        name="mixer",
    )(
        latent, context, cond.reshape(lines(cond)), cond_ctx.reshape(lines(cond)), wsh.T, wsc.T, wga.T, gain.reshape(lines(gain)),
        pz.T, px.T, pb, pc, pdt, cx, cb, cc, dtb.reshape(1, 2), dlog.reshape(1, 2), hg.reshape(1, -1), po.T,
    )


def build(mesh, sizes):
    Z, Y, X = sizes
    torus = Mesh(mesh.devices.reshape(Z, Y, X, 2), SP_TP)
    in_specs = (
        P(SP_TP, None), P("sp", None), P("sp"), P("sp"), P("sp", TP), P("sp", TP), P("sp", TP), P(),
        P(None, TP), P(None, TP), P(None, TP), P(None, TP), P(), P(None, TP), P(None, TP), P(None, TP),
        P(TP), P(TP), P(TP), P(None, TP),
    )
    return jax.shard_map(
        functools.partial(per_device, sizes), mesh=torus, in_specs=in_specs, out_specs=P(SP_TP, None), check_vma=False
    )


def solution(mesh):
    return build(mesh, (mesh.shape["sp"], 8, 4))
```

time: 112 us -> 88.9 us (0.79)
  Pallas kernels: 100 us -> 87.3 us
  local copies, waits for them, and re-layouts: 11.4 us -> 1.39 us
    pallas_call x1, Pallas kernels: 100 us -> 87.3 us  [per_device(): pl.pallas_call(functools.partial(kernel, sizes), out_shape=jax.ShapeDtype...]
    unnamed x39 -> x1, local copies, waits for them, and re-layouts: 10.7 us -> 1.39 us
where the time goes in v2:
time: 88.9 us; the launch traced here: 88.7 us
  Pallas kernels  87.3 us (98%)
  local copies, waits for them, and re-layouts  1.39 us (2%)
    pallas_call x1, Pallas kernels, per_device(): pl.pallas_call(functools.partial(kernel, sizes), out_shape=jax.ShapeDtype...  87.3 us

profile of v2, /device:TPU:1, one launch (start us, length us, event | category | flops | bytes accessed | tf_op | source)
XLA Modules:
  0.0 88.7 jit_solution(6774599075034632430)
XLA Ops:
  0.0 87.3 %mixer.1 = bf16[4,4096]{1,0:T(4,128)(2,1)} custom-call(bf16[4,4096]{1,0:T(4,128)(2,1)} %lat_h.1, bf16[16,4096]{1,0:T(8,128)(2,1)} %ctx_h.1, bf16[2,128]{1,0:T(2,128)(2,1)} %bitcast.19, bf16[2,128]{1,0:T(2,128)(2,1)} %bitcast.20, bf16[64,256]{1,0:T(8,128)(2,1)} %bitcast.15, bf16[64,256]{1,0:T(8,128)(2,1)} %bitcast.16, bf16[64,256]{1,0:T(8,128)(2,1)} %bitcast.17, ...), custom_call_target="tpu_custom_call" | custom-call | tf_op jit(solution)/shard_map/mixer/pallas_call | solution.py:622
  87.3 1.4 %copy.22 = bf16[4,4096]{1,0:T(4,128)(2,1)} copy(bf16[4,4096]{1,0:T(4,128)(2,1)} %mixer.1) | data formatting | bytes 65536

commit v3 on v2

--- a/solution.py
+++ b/solution.py
@@ -46,15 +46,15 @@
     cx_ref, cb_ref, cc_ref, dtb_ref, dlog_ref, hg_ref,
     wcat, wxz, wot, wo, latbuf, pbuf, psend, mpair, mpair_r, mbuf, sbuf, acc, acco,
     cbuf, ebuf, esend, lbuf, snd, rst, osend, orecv, obuf, ubuf, rbuf, cst, ssq,
-    wsem, wosem, worsem, pss, prs, mps, mpr, m1s, m1r, m2s, m2r, lgs, lgy, lgx, ld_s, ldr,
-    css, csr, es, er, ls_, lr_, sts, str_, ops, opr, ogs, ogy, ogx, us, ur,
+    wsem, wosem, worsem, pss, prs, mps, mpr, m1s, m1r, m2s, m2r, lgs, lgy, lgx, lga, lgb, ld_s, ldr, lda,
+    css, csr, es, er, ls_, lr_, sts, str_, ops, opr, ogs, ogy, ogx, oga, ogb, us, ur,
 ):
     Z, Y, X = sizes
     NC = Y * X
     HC = NC // 2
     D = lat_ref.shape[1]
     HD = D // 2
-    HQ = D // 4
+    LT = HD // 128
     T = NC * 8
     TH = T // 2
     CZ = ctx_ref.shape[0]
@@ -79,6 +79,31 @@
 
     partner = {"tp_2": 1 - c}
 
+    bar = pltpu.get_barrier_semaphore()
+
+    def hello(dev):
+        pl.semaphore_signal(bar, inc=1, device_id=dev, device_id_type=MESH_ID)
+
+    def greet_z(i, carry):
+        hello({"sp": lax.rem(z + i, Z)})
+        return carry
+
+    def greet_row(i, carry):
+        yy = lax.rem(y + i, Y)
+        for d in range(X):
+            xx = lax.rem(x + d, X)
+            hello({"tp_0": yy, "tp_1": xx})
+            hello({"tp_0": yy, "tp_1": xx, "tp_2": 1 - c})
+        return carry
+
+    lax.fori_loop(1, Z, greet_z, 0)
+    hello(partner)
+    for d in range(1, X):
+        xx = lax.rem(x + d, X)
+        hello({"tp_1": xx})
+        hello({"tp_1": xx, "tp_2": 1 - c})
+    lax.fori_loop(1, Y, greet_row, 0)
+
     wot_own = wot.at[pl.ds(pl.multiple_of(c * 64, 64), 64)]
     moves = [
         (lat_h, lat_ref), (wsh_h, wsh_ref), (wsc_h, wsc_ref), (wga_h, wga_ref), (cond_h, cond_ref), (condc_h, condc_ref),
@@ -91,31 +116,6 @@
     for load in loads:
         load.start()
 
-    bar = pltpu.get_barrier_semaphore()
-
-    def hello(dev):
-        pl.semaphore_signal(bar, inc=1, device_id=dev, device_id_type=MESH_ID)
-
-    def greet_z(i, carry):
-        hello({"sp": lax.rem(z + i, Z)})
-        return carry
-
-    def greet_row(i, carry):
-        yy = lax.rem(y + i, Y)
-        for d in range(X):
-            xx = lax.rem(x + d, X)
-            hello({"tp_0": yy, "tp_1": xx})
-            hello({"tp_0": yy, "tp_1": xx, "tp_2": 1 - c})
-        return carry
-
-    hello(partner)
-    for d in range(1, X):
-        xx = lax.rem(x + d, X)
-        hello({"tp_1": xx})
-        hello({"tp_1": xx, "tp_2": 1 - c})
-    lax.fori_loop(1, Y, greet_row, 0)
-    lax.fori_loop(1, Z, greet_z, 0)
-
     nt = (((1,), (1,)), ((), ()))
     tn = (((0,), (0,)), ((), ()))
 
@@ -157,47 +157,91 @@
     def near(n):
         return [d for k in range(1, (n + 1) // 2) for d in (k, n - k)] + ([n // 2] if n % 2 == 0 else [])
 
-    def gather(buf, ssem, ysem, xsem, middle, row_done):
-        def x_send(row):
-            slot = buf.at[row * X + x]
+    def groups(buf):
+        n = buf.shape[1]
+        few = max(1, n // 8)
+        return n - few, few
+
+    def gather(buf, ssem, ysem, xsem, asem, bsem, middle, row_done):
+        nb, na = groups(buf)
+
+        def copy(k, part, sem, dev):
+            ref = buf.at[k, pl.ds(0, nb)] if part == 0 else buf.at[k, pl.ds(nb, na)]
+            return remote(ref, ref, ssem, sem, dev)
+
+        def along_x(row, part, sem_of):
             for d in near(X):
-                remote(slot, slot, ssem, xsem.at[row], {"tp_1": lax.rem(x + d, X)}).start()
+                copy(row * X + x, part, sem_of, {"tp_1": lax.rem(x + d, X)}).start()
+
+        def along_y(col, part, sem_of):
+            for d in near(Y):
+                copy(y * X + col, part, sem_of, {"tp_0": lax.rem(y + d, Y)}).start()
 
         def x_take(row):
-            drain(buf, X - 1, xsem.at[row])
+            ref = buf.at[pl.ds(0, X - 1), pl.ds(0, nb)]
+            pltpu.make_async_copy(ref, ref, xsem.at[row]).wait()
             row_done(row)
 
-        own = buf.at[chip]
-        x_send(y)
-        for d in near(Y):
-            remote(own, own, ssem, ysem.at[y], {"tp_0": lax.rem(y + d, Y)}).start()
+        cols = [lax.rem(x + X - d, X) for d in near(X)]
+
+        def turn():
+            col = cols.pop(0)
+            copy(y * X + col, 1, asem.at[col], partner).wait_recv()
+            along_y(col, 1, bsem)
+
+        along_x(y, 1, asem.at[x])
+        along_y(x, 0, ysem.at[y])
+        along_x(y, 0, xsem.at[y])
+        along_y(x, 1, bsem)
         rows = [y]
         for n, d in enumerate(near(Y)):
             row = lax.rem(y + Y - d, Y)
-            slot = buf.at[row * X + x]
-            remote(slot, slot, ssem, ysem.at[row], partner).wait_recv()
-            x_send(row)
+            copy(row * X + x, 0, ysem.at[row], partner).wait_recv()
+            along_x(row, 0, xsem.at[row])
             rows.append(row)
+            if n == 1:
+                while len(cols) > 1:
+                    turn()
+            if n == 3:
+                while cols:
+                    turn()
             if n in (3, 5):
                 x_take(rows.pop(0))
+        while cols:
+            turn()
         middle()
         for row in rows:
             x_take(row)
+        ref = buf.at[pl.ds(0, NC - X), pl.ds(0, na)]
+        pltpu.make_async_copy(ref, ref, bsem).wait()
+
+    def gather_drain(buf, sem):
+        drain(buf, NC - 1, sem)
 
     mine = latbuf.at[c]
     other = latbuf.at[1 - c]
 
+    nb_lat, na_lat = groups(mine)
+
     def squares(h, row):
         for j in range(X):
-            v = latbuf[h, row * X + j].astype(F32)
-            v = v * v
-            t = v[0] + v[1]
-            ssq[h, row * X + j] = sum(t[:, k * 128 : k * 128 + 128] for k in range(HQ // 128))
+            v = latbuf[h, row * X + j, 0:nb_lat].astype(F32)
+            ssq[h, row * X + j] = jnp.sum(v * v, axis=0)
+
+    def squares_last(h):
+        total = ssq[h]
+        for k in range(na_lat):
+            v = latbuf[h, :, nb_lat + k].astype(F32)
+            total = total + v * v
+        return total
 
     late = []
 
     def row_of(ref, row):
-        return ref.at[pl.ds(row * X, X)]
+        return ref.at[pl.ds(row * X, X), pl.ds(0, nb_lat)]
+
+    def last_of(ref):
+        return ref.at[pl.ds(0, NC), pl.ds(nb_lat, na_lat)]
 
     def from_partner():
         row = late.pop(0)
@@ -215,8 +259,8 @@
     got = pbuf[...].astype(F32)
     own = jnp.where(first_core, lat[:, :HD], lat[:, HD:])
     block = jnp.concatenate([jnp.where(first_core, own, got), jnp.where(first_core, got, own)], 0).astype(BF16)
-    latbuf[c, chip, 0] = block[:, :HQ]
-    latbuf[c, chip, 1] = block[:, HQ:]
+    for k in range(LT):
+        latbuf[c, chip, k] = block[:, k * 128 : k * 128 + 128]
 
     mp.wait_recv()
     mbuf[z] = mpair[...] + mpair_r[...]
@@ -268,19 +312,23 @@
 
         wocopy.start()
 
-    gather(mine, lgs, lgy, lgx, middle, to_partner)
+    gather(mine, lgs, lgy, lgx, lga, lgb, middle, to_partner)
+    last = remote(last_of(mine), last_of(mine), ld_s, lda, partner)
+    last.start()
     r_ctx = scale_of[0]
 
     while late:
         from_partner()
-    tot = (ssq[0] + ssq[1]).reshape(T, 128)
+    own_squares = squares_last(c)
+    last.wait_recv()
+    tot = (own_squares + squares_last(1 - c)).reshape(T, 128)
     r_lat = lax.rsqrt(jnp.sum(tot, axis=1, keepdims=True) / D + EPS)
 
     drain(sbuf, NC - 1, m2r)
 
-    CH = min(4, NC // 4)
+    CH = min(4, HC)
     KB = CH * 128
-    NQ = HQ // KB
+    NQ = HD // KB
 
     def scales(i, row):
         return jnp.concatenate([sbuf[i * CH + j][row : row + 1] for j in range(CH)], 1)
@@ -291,18 +339,21 @@
         return jnp.concatenate([gains_all[i * CH + j : i * CH + j + 1] for j in range(CH)], 1)
 
     def chunk(i):
-        return i // (2 * NQ), i // NQ % 2, i % NQ * KB, i * KB
+        return i // NQ, i % NQ * CH, i * KB
+
+    def tiles(h, slot, k):
+        return jnp.concatenate([latbuf[h, slot, k + j].astype(F32) for j in range(CH)], 1)
 
     def small(i, carry):
-        h, q, off, at = chunk(i)
+        h, k, at = chunk(i)
         gains = gains_of(i)
         gs = gains * (1.0 + scales(i, 1))
         sh = scales(i, 0)
         gsc = gains * (1.0 + scales(i, 3))
         shc = scales(i, 2)
         vc = ctx_ref[:, pl.ds(at, KB)].astype(F32) * r_ctx * gsc + shc
-        v0 = latbuf[h, 0, q, :, pl.ds(off, KB)].astype(F32) * r_lat[0:8] * gs + sh
-        v1 = latbuf[h, NC - 1, q, :, pl.ds(off, KB)].astype(F32) * r_lat[T - 8 : T] * gs + sh
+        v0 = tiles(h, 0, k) * r_lat[0:8] * gs + sh
+        v1 = tiles(h, NC - 1, k) * r_lat[T - 8 : T] * gs + sh
         rows = jnp.concatenate([vc, v0, v1], 0).astype(BF16)
         return carry + jnp.dot(rows, wcat[pl.ds(at, KB), :], preferred_element_type=F32)
 
@@ -335,10 +386,10 @@
         c_last.start()
 
     def main(i, total):
-        h, q, off, at = chunk(i)
+        h, k, at = chunk(i)
         gs = gains_of(i) * (1.0 + scales(i, 1))
         sh = scales(i, 0)
-        v = latbuf[h, :, q, :, pl.ds(off, KB)].astype(F32).reshape(T, KB)
+        v = jnp.concatenate([latbuf[h, :, k + j].astype(F32).reshape(T, 128) for j in range(CH)], 1)
         rows = (v * r_lat * gs + sh).astype(BF16)
         return total + jnp.dot(rows, wcat[pl.ds(at, KB), :], preferred_element_type=F32)
 
@@ -515,15 +566,20 @@
     keep = jnp.where(first_core, heads[0:TH], heads[TH:T])
     op.wait_recv()
     joined = (keep + orecv[...].astype(F32)).astype(BF16)
-    obuf[chip] = joined
+    obuf[chip] = joined.reshape(TH // 8, 8, 128)
     acco[...] = jnp.zeros_like(acco)
 
+    nb_out, _ = groups(obuf)
+    TB = nb_out * 8
+
     def row_dot(row):
-        rows = jnp.concatenate([obuf[row * X + j] for j in range(X)], 1)
+        rows = jnp.concatenate([obuf[row * X + j, 0:nb_out].reshape(TB, 128) for j in range(X)], 1)
         span = pl.ds(pl.multiple_of(row * (X * 128), 128), X * 128)
-        acco[...] += jnp.dot(rows, wo[span, :], preferred_element_type=F32)
-
-    gather(obuf, ogs, ogy, ogx, lambda: None, row_dot)
+        acco[0:TB] += jnp.dot(rows, wo[span, :], preferred_element_type=F32)
+
+    gather(obuf, ogs, ogy, ogx, oga, ogb, lambda: None, row_dot)
+    rest = jnp.concatenate([obuf[k, nb_out:].reshape(TH - TB, 128) for k in range(NC)], 1)
+    acco[TB:] = jnp.dot(rest, wo[...], preferred_element_type=F32)
     upd = acco[...] * mpair[4:5]
     ubuf[...] = upd.reshape(TH // 8, 8, 128).astype(BF16)
 
@@ -578,7 +634,7 @@
     op.wait_send()
     drain(mbuf, Z - 1, m1s)
     drain(sbuf, NC - 1, m2s)
-    drain(mine, NC - 1, lgs)
+    gather_drain(mine, lgs)
     drain(mine, NC, ld_s)
 
     @pl.when(z > 0)
@@ -591,7 +647,7 @@
 
     drain(lbuf, Z - 1, ls_)
     drain(rst, Z - 1, sts)
-    drain(obuf, NC - 1, ogs)
+    gather_drain(obuf, ogs)
 
     @pl.when(in_half)
     def _():
@@ -629,13 +685,13 @@
             V((64, D // Z), BF16), V((64, D // Z), BF16), V((64, D // Z), BF16), V(lines(gain), BF16),
             V((3, 64), BF16), V((3, 128), BF16), V((3, 128), BF16), V((1, 2), F32), V((1, 2), F32), V((1, 64), BF16),
             V((D, 512), BF16), V((128, D), BF16), V((128, D), BF16), V((D, 128), BF16),
-            V((2, NC, 2, 8, D // 4), BF16), V((4, D // 2), BF16), V((4, D // 2), BF16), V((5, 128), F32), V((5, 128), F32),
+            V((2, NC, D // 256, 8, 128), BF16), V((4, D // 2), BF16), V((4, D // 2), BF16), V((5, 128), F32), V((5, 128), F32),
             V((Z, 5, 128), F32), V((NC, 4, 128), F32), V((T, 512), F32), V((T // 2, 128), F32),
             V((Z, CZ, 256), BF16), V((2, 8, 384), BF16), V((2, 8, 384), BF16), V((Z, 1, 128), F32),
             V((2, 64, 128), BF16), V((Z, 64, 128), BF16), V((T // 2, 128), BF16), V((T // 2, 128), BF16),
-            V((NC, T // 2, 128), BF16), V((T // 16, 8, 128), BF16), V((NC, 8, 128), BF16), V((128, 128), F32), V((2, NC, 8, 128), F32),
-            S((20,)), one, one, one, one, one, one, one, one, one, one, one, S((Y,)), S((Y,)), one, S((Y,)),
-            S((2,)), one, S((2,)), S((2,)), one, one, one, one, one, one, one, S((Y,)), S((Y,)), one, one,
+            V((NC, T // 16, 8, 128), BF16), V((T // 16, 8, 128), BF16), V((NC, 8, 128), BF16), V((128, 128), F32), V((2, NC, 8, 128), F32),
+            S((20,)), one, one, one, one, one, one, one, one, one, one, one, S((Y,)), S((Y,)), S((X,)), one, one, S((Y,)), one,
+            S((2,)), one, S((2,)), S((2,)), one, one, one, one, one, one, one, S((Y,)), S((Y,)), S((X,)), one, one, one,
         ],
         compiler_params=pltpu.CompilerParams(collective_id=0, has_side_effects=True),
         name="mixer",

time: 88.9 us -> 86.6 us (0.974)
  Pallas kernels: 87.3 us -> 85 us
    pallas_call x1, Pallas kernels: 87.3 us -> 85 us  [per_device(): pl.pallas_call(functools.partial(kernel, sizes), out_shape=jax.ShapeDtype...]
where the time goes in v3:
time: 86.6 us; the launch traced here: 86.4 us
  Pallas kernels  85 us (98%)
  local copies, waits for them, and re-layouts  1.39 us (2%)
    pallas_call x1, Pallas kernels, per_device(): pl.pallas_call(functools.partial(kernel, sizes), out_shape=jax.ShapeDtype...  85 us

profile of v3, /device:TPU:1, one launch (start us, length us, event | category | flops | bytes accessed | tf_op | source)
XLA Modules:
  0.0 86.4 jit_solution(5274990066483261768)
XLA Ops:
  0.0 85.0 %mixer.1 = bf16[4,4096]{1,0:T(4,128)(2,1)} custom-call(bf16[4,4096]{1,0:T(4,128)(2,1)} %lat_h.1, bf16[16,4096]{1,0:T(8,128)(2,1)} %ctx_h.1, bf16[2,128]{1,0:T(2,128)(2,1)} %bitcast.19, bf16[2,128]{1,0:T(2,128)(2,1)} %bitcast.20, bf16[64,256]{1,0:T(8,128)(2,1)} %bitcast.15, bf16[64,256]{1,0:T(8,128)(2,1)} %bitcast.16, bf16[64,256]{1,0:T(8,128)(2,1)} %bitcast.17, ...), custom_call_target="tpu_custom_call" | custom-call | tf_op jit(solution)/shard_map/mixer/pallas_call | solution.py:678
  85.0 1.4 %copy.22 = bf16[4,4096]{1,0:T(4,128)(2,1)} copy(bf16[4,4096]{1,0:T(4,128)(2,1)} %mixer.1) | data formatting | bytes 65536
